TPU v7x, 256 devices: a whole 4x4x8 slice. The times are simulated.
256 devices in a mesh: sp: 64 (over z, x, core), tp: 4 (over y).
Axes of the slice: x: 4, y: 4, z: 8, core: 2. Of those that a mesh axis runs over, the one named last changes fastest.
Arguments:
- residual: bfloat16 [24576, 2048], P('sp', 'tp'), may hold values from -6 to 6
- query_nope: bfloat16 [24576, 4096], P('sp', 'tp'), may hold values from -9 to 9
- query_rope: bfloat16 [24576, 2048], P('sp', 'tp'), may hold values from -600 to 600
- latent: bfloat16 [24576, 512], P('sp'), may hold values from -6 to 6
- rope_key: bfloat16 [24576, 64], P('sp'), may hold values from -6 to 6
- doc_ids: int32 [24576], P('sp'), may hold values from 0 to 31, never falling along the last dimension, each value on 1 to 1152 neighbouring positions
- key_up: bfloat16 [512, 4096], P(None, 'tp'), may hold values from -0.25 to 0.25
- value_up: bfloat16 [512, 4096], P(None, 'tp'), may hold values from -0.25 to 0.25
- out_proj: bfloat16 [4096, 2048], P('tp'), may hold values from -0.375 to 0.375
- norm1_gain: bfloat16 [2048], P('tp'), may hold values from 0.099609375 to 1.8984375
- norm1_bias: bfloat16 [2048], P('tp'), may hold values from -3 to 3
- ffn_gate: bfloat16 [2048, 5632], P('sp', 'tp'), may hold values from -0.125 to 0.125
- ffn_value: bfloat16 [2048, 5632], P('sp', 'tp'), may hold values from -0.125 to 0.125
- conv_gate: bfloat16 [3, 5632], P(None, 'tp'), may hold values from -3.5 to 3.5
- conv_value: bfloat16 [3, 5632], P(None, 'tp'), may hold values from -3.5 to 3.5
- ffn_down: bfloat16 [5632, 2048], P('tp', 'sp'), may hold values from -0.15625 to 0.15625
- norm2_gain: bfloat16 [2048], P('tp'), may hold values from 0.099609375 to 1.8984375
- norm2_bias: bfloat16 [2048], P('tp'), may hold values from -3 to 3
Outputs:
- layer_out: bfloat16 [24576, 2048], P('sp', 'tp')
Inputs may be any that keep to these rules, and one draw needn't show every extreme that they name: `doc_ids`: document numbers never fall along the positions; each document holds 1 to 1152 positions, and one holds exactly 1152.
All inputs are finite; a program needn't handle non-finite values.
Results may differ from a plain program's by a relative error of at most 0.014.
Values may be sent and summed in bfloat16 or wider, within the bound.
A program may use at most 128 MiB of HBM per device.

v0:
```python
import jax
import jax.numpy as jnp
from jax import lax
from jax.sharding import PartitionSpec as P

D = 2048
NOPE = 128
ROPE = 64
VDIM = 128
CONV = 3
REACH = 3


norm_eps = 1e-05
residual_scale = 8.0**0.25
rope_base_freq = 10000.0
masked_score = -1e30


def passed_along(value, axis, by):
    count = lax.axis_size(axis)
    pairs = [(i, i + by) for i in range(count) if 0 <= i + by < count]
    return lax.ppermute(value, axis, pairs)


def split_up(value, dim, count):
    lengths = value.shape
    parts = value.reshape(*lengths[:dim], count, lengths[dim] // count, *lengths[dim + 1 :])
    return jnp.moveaxis(parts, dim, 0)


def sum_at_owner(value, axis, dim):
    parts = split_up(value, dim, lax.axis_size(axis))
    arrived = lax.all_to_all(parts, axis, split_axis=0, concat_axis=0, tiled=True)
    return arrived.astype(jnp.float32).sum(axis=0)


def from_everyone(value, axis):
    copies = jnp.broadcast_to(value, (lax.axis_size(axis), *value.shape))
    return lax.all_to_all(copies, axis, split_axis=0, concat_axis=0, tiled=True)


def over_copies(value, axis):
    everything = from_everyone(value, axis)
    return jnp.sum(everything, axis=0)


def in_one(arrays, axis):
    ends = [0]
    for a in arrays:
        ends.append(ends[-1] + a.size)
    running = over_copies(jnp.concatenate([a.ravel() for a in arrays]), axis)
    return tuple((running[b:e].reshape(a.shape) for a, b, e in zip(arrays, ends, ends[1:])))


def laid_out(parts, dim):
    parts = jnp.moveaxis(parts, 0, dim)
    lengths = parts.shape
    return parts.reshape(*lengths[:dim], lengths[dim] * lengths[dim + 1], *lengths[dim + 2 :])


def gathered_copies(value, axis, dim):
    parts = from_everyone(value, axis)
    return laid_out(parts, dim)


def sent_together(arrays, axis, dim, along):
    widths = [a.shape[along] for a in arrays]
    both = jnp.concatenate(arrays, axis=along)
    out = lax.all_gather(both, axis, axis=dim, tiled=True)
    return tuple(jnp.split(out, [sum(widths[:k]) for k in range(1, len(widths))], axis=along))


def tables(positions):
    frequencies = 1.0 / rope_base_freq ** (jnp.arange(0, ROPE, 2, dtype=jnp.float32) / ROPE)
    angles = positions.astype(jnp.float32)[:, None] * frequencies[None, :]
    return (jnp.cos(angles), jnp.sin(angles))


def rotate(vectors, cosine, sine_table):
    half_width = vectors.shape[-1] // 2
    front_half = vectors[..., :half_width]
    back_half = vectors[..., half_width:]
    return jnp.concatenate(
        [
            front_half * cosine - back_half * sine_table,
            front_half * sine_table + back_half * cosine,
        ],
        axis=-1,
    )


def finish(mixed, totals, gain_row, bias_row):
    row_mean = totals[0][:, None] / D
    row_power = totals[1][:, None] / D
    return (mixed - row_mean) * lax.rsqrt(
        row_power - row_mean * row_mean + norm_eps
    ) * gain_row.astype(jnp.float32) + bias_row.astype(jnp.float32)


def local(
    residual,
    query_nope,
    query_rope,
    latent,
    rope_key,
    doc_ids,
    key_up,
    value_up,
    out_proj,
    norm1_gain,
    norm1_bias,
    ffn_gate,
    ffn_value,
    conv_gate,
    conv_value,
    ffn_down,
    norm2_gain,
    norm2_bias,
):
    row_count = latent.shape[0]
    head_count = query_nope.shape[1] // NOPE
    local_units = ffn_gate.shape[1]
    rim_rows = CONV - 1
    offset = lax.axis_index("sp") * row_count
    positions = offset + jnp.arange(row_count, dtype=jnp.int32)
    cosine, sine_table = tables(positions)
    turned_key = rotate(rope_key.astype(jnp.float32), cosine, sine_table).astype(jnp.bfloat16)
    turned_query = rotate(
        query_rope.astype(jnp.float32).reshape(row_count, head_count, ROPE),
        cosine[:, None],
        sine_table[:, None],
    ).astype(jnp.bfloat16)
    latent_list = []
    rim_list = []
    doc_list = []
    for shift_step in range(REACH, 0, -1):
        far_latent, far_key, far_doc = passed_along((latent, turned_key, doc_ids), "sp", shift_step)
        latent_list.append(far_latent)
        rim_list.append(far_key)
        doc_list.append(far_doc)
    win_latent = jnp.concatenate(latent_list + [latent], 0)
    win_key = jnp.concatenate(rim_list + [turned_key], 0)
    win_doc = jnp.concatenate(doc_list + [doc_ids], 0)
    key_rows = jnp.dot(win_latent, key_up, preferred_element_type=jnp.float32).astype(jnp.bfloat16)
    values = jnp.dot(win_latent, value_up, preferred_element_type=jnp.float32).astype(jnp.bfloat16)
    window = key_rows.shape[0]
    key_pos = offset - REACH * row_count + jnp.arange(window, dtype=jnp.int32)
    allowed = (
        (key_pos[None, :] <= positions[:, None])
        & (key_pos[None, :] >= 0)
        & (win_doc[None, :] == doc_ids[:, None])
    )
    scale = (NOPE + ROPE) ** (-0.5)
    scores = jnp.einsum(
        "qhd,khd->hqk",
        query_nope.reshape(row_count, head_count, NOPE),
        key_rows.reshape(window, head_count, NOPE),
        preferred_element_type=jnp.float32,
    )
    scores = scores + jnp.einsum(
        "qhr,kr->hqk", turned_query, win_key, preferred_element_type=jnp.float32
    )
    scores = jnp.where(allowed[None], scores * scale, masked_score)
    row_max = jnp.max(scores, -1, keepdims=True)
    weights = jnp.exp(scores - row_max)
    weights = (weights / jnp.sum(weights, -1, keepdims=True)).astype(jnp.bfloat16)
    attended = jnp.einsum(
        "hqk,khd->qhd",
        weights,
        values.reshape(window, head_count, VDIM),
        preferred_element_type=jnp.float32,
    )
    attended = attended.astype(jnp.bfloat16).reshape(row_count, head_count * VDIM)
    head_terms = jnp.dot(attended, out_proj, preferred_element_type=jnp.float32)
    projected = sum_at_owner(head_terms.astype(jnp.bfloat16), "tp", 1)
    mixed_one = residual_scale * residual.astype(jnp.float32) + projected
    totals_one = in_one((jnp.sum(mixed_one, 1), jnp.sum(mixed_one * mixed_one, 1)), "tp")
    normed = finish(mixed_one, totals_one, norm1_gain, norm1_bias).astype(jnp.bfloat16)
    full_rows = gathered_copies(normed, "tp", 1)
    shard_piece = sent_together((ffn_gate, ffn_value), "sp", 0, 1)
    gate_sum = jnp.dot(full_rows, shard_piece[0], preferred_element_type=jnp.float32)
    value_sum = jnp.dot(full_rows, shard_piece[1], preferred_element_type=jnp.float32)
    gate_pre = gate_sum.astype(jnp.bfloat16)
    value_pre = value_sum.astype(jnp.bfloat16)
    tail_gate, tail_value, tail_doc = passed_along(
        (
            gate_pre[row_count - rim_rows :],
            value_pre[row_count - rim_rows :],
            doc_ids[row_count - rim_rows :],
        ),
        "sp",
        1,
    )
    ext_gate = jnp.concatenate([tail_gate, gate_pre], 0)
    ext_value = jnp.concatenate([tail_value, value_pre], 0)
    ext_doc = jnp.concatenate([tail_doc, doc_ids], 0)
    gate_mix = jnp.zeros((row_count, local_units), jnp.float32)
    value_mix = jnp.zeros((row_count, local_units), jnp.float32)
    for tap_index in range(CONV):
        valid_tap = (
            (ext_doc[tap_index : tap_index + row_count] == doc_ids)
            & (positions - rim_rows + tap_index >= 0)
        ).astype(jnp.float32)[:, None]
        gate_mix = (
            gate_mix
            + conv_gate[tap_index].astype(jnp.float32)
            * ext_gate[tap_index : tap_index + row_count].astype(jnp.float32)
            * valid_tap
        )
        value_mix = (
            value_mix
            + conv_value[tap_index].astype(jnp.float32)
            * ext_value[tap_index : tap_index + row_count].astype(jnp.float32)
            * valid_tap
        )
    hidden = (value_mix * jax.nn.gelu(gate_mix)).astype(jnp.bfloat16)
    unit_terms = jnp.dot(
        hidden,
        lax.all_gather(ffn_down, "sp", axis=1, tiled=True),
        preferred_element_type=jnp.float32,
    )
    ffn_out = sum_at_owner(unit_terms.astype(jnp.bfloat16), "tp", 1)
    mixed_two = residual_scale * normed.astype(jnp.float32) + ffn_out
    totals_two = in_one((jnp.sum(mixed_two, 1), jnp.sum(mixed_two * mixed_two, 1)), "tp")
    return finish(mixed_two, totals_two, norm2_gain, norm2_bias).astype(jnp.bfloat16)


def solution(mesh):
    placed = (
        P("sp", "tp"),
        P("sp", "tp"),
        P("sp", "tp"),
        P("sp", None),
        P("sp", None),
        P("sp"),
        P(None, "tp"),
        P(None, "tp"),
        P("tp", None),
        P("tp"),
        P("tp"),
        P("sp", "tp"),
        P("sp", "tp"),
        P(None, "tp"),
        P(None, "tp"),
        P("tp", "sp"),
        P("tp"),
        P("tp"),
    )
    return jax.shard_map(
        local, mesh=mesh, in_specs=placed, out_specs=P("sp", "tp"), check_vma=False
    )
```

profile of v0, /device:TPU:6, one launch (start us, length us, event | category | flops | bytes accessed | tf_op | source)
XLA Modules:
  0.0 246.4 jit_solution(11918921222139653919)
XLA Ops:
  6.5 1.7 pad_maximum_fusion.2
  8.3 0.7 all-gather.5.cloned.1.call-update
  9.1 0.8 convert_element_type.119
  9.9 0.3 subtract_convert_fusion.1
  10.2 3.2 %collective-permute-start.6 = (bf16[384,64]{0,1:T(8,128)(2,1)S(1)}, bf16[384,64]{0,1:T(8,128)(2,1)S(1)}, u32[]{:S(2)}, u32[]{:S(2)}) collective-permute-start(bf16[384,64]{0,1:T(8,128)(2,1)S(1)} %pad_maximum_fusion.3), channel_id=1, source_target_pairs={{0,12},{4,16},{8,20},{12,24},{16,28},{20,32},{24,36},{28,40},{32,4... | collective-permute-start | bytes 147464 | tf_op jit(solution)/shard_map/ppermute | solution.py:23
  13.4 3.4 %collective-permute-start.7 = (bf16[384,64]{0,1:T(8,128)(2,1)S(1)}, bf16[384,64]{0,1:T(8,128)(2,1)S(1)}, u32[]{:S(2)}, u32[]{:S(2)}) collective-permute-start(bf16[384,64]{0,1:T(8,128)(2,1)S(1)} %pad_maximum_fusion.3), channel_id=1, source_target_pairs={{0,8},{4,12},{8,16},{12,20},{16,24},{20,28},{24,32},{28,36},{32,40... | collective-permute-start | bytes 147464 | tf_op jit(solution)/shard_map/ppermute | solution.py:23
  16.8 4.0 %collective-permute-start.3 = (s32[384]{0:T(512)}, s32[384]{0:T(512)S(1)}, u32[]{:S(2)}, u32[]{:S(2)}) collective-permute-start(s32[384]{0:T(512)} %param.23), channel_id=1, source_target_pairs={{0,12},{4,16},{8,20},{12,24},{16,28},{20,32},{24,36},{28,40},{32,4... | collective-permute-start | bytes 4616 | tf_op jit(solution)/shard_map/ppermute | solution.py:23
  20.8 3.1 %collective-permute-start.4 = (s32[384]{0:T(512)}, s32[384]{0:T(512)S(1)}, u32[]{:S(2)}, u32[]{:S(2)}) collective-permute-start(s32[384]{0:T(512)} %param.23), channel_id=1, source_target_pairs={{0,8},{4,12},{8,16},{12,20},{16,24},{20,28},{24,32},{28,36},{32,40... | collective-permute-start | bytes 4616 | tf_op jit(solution)/shard_map/ppermute | solution.py:23
  24.0 3.0 %collective-permute-start.5 = (s32[384]{0:T(512)}, s32[384]{0:T(512)S(1)}, u32[]{:S(2)}, u32[]{:S(2)}) collective-permute-start(s32[384]{0:T(512)} %param.23), channel_id=1, source_target_pairs={{0,4},{4,8},{8,12},{12,16},{16,20},{20,24},{24,28},{28,32},{32,36}... | collective-permute-start | bytes 4616 | tf_op jit(solution)/shard_map/ppermute | solution.py:23
  26.9 1.2 copy.44
  28.3 4.8 %collective-permute-start = (bf16[384,512]{1,0:T(8,128)(2,1)S(1)}, bf16[384,512]{1,0:T(8,128)(2,1)S(1)}, u32[]{:S(2)}, u32[]{:S(2)}) collective-permute-start(bf16[384,512]{1,0:T(8,128)(2,1)S(1)} %copy-done.4), channel_id=1, source_target_pairs={{0,12},{4,16},{8,20},{12,24},{16,28},{20,32},{24,36},{28,40},{32,4... | collective-permute-start | bytes 1179656 | tf_op jit(solution)/shard_map/ppermute | solution.py:23
  33.1 2.5 %collective-permute-start.1 = (bf16[384,512]{1,0:T(8,128)(2,1)S(1)}, bf16[384,512]{1,0:T(8,128)(2,1)S(1)}, u32[]{:S(2)}, u32[]{:S(2)}) collective-permute-start(bf16[384,512]{1,0:T(8,128)(2,1)S(1)} %copy-done.4), channel_id=1, source_target_pairs={{0,8},{4,12},{8,16},{12,20},{16,24},{20,28},{24,32},{28,36},{32,40... | collective-permute-start | bytes 1179656 | tf_op jit(solution)/shard_map/ppermute | solution.py:23
  35.6 2.1 collective-permute-start.2
  37.7 1.4 compare_and_fusion
  39.1 7.0 %collective-permute-done = bf16[384,512]{1,0:T(8,128)(2,1)S(1)} collective-permute-done((bf16[384,512]{1,0:T(8,128)(2,1)S(1)}, bf16[384,512]{1,0:T(8,128)(2,1)S(1)}, u32[]{:S(2)}, u32[]{:S(2)}) %collective-permute-start) | collective-permute-done | bytes 393248 | tf_op jit(solution)/shard_map/ppermute | solution.py:23
  46.1 1.9 collective-permute-start.8
  48.1 7.3 %collective-permute-done.1 = bf16[384,512]{1,0:T(8,128)(2,1)S(1)} collective-permute-done((bf16[384,512]{1,0:T(8,128)(2,1)S(1)}, bf16[384,512]{1,0:T(8,128)(2,1)S(1)}, u32[]{:S(2)}, u32[]{:S(2)}) %collective-permute-start.1) | collective-permute-done | bytes 393248 | tf_op jit(solution)/shard_map/ppermute | solution.py:23
  55.6 1.8 convolution_convert_fusion
  57.4 8.3 %fusion.40 = f32[8,1536,384]{2,1,0:T(8,128)} fusion(bf16[1536,8,128]{0,2,1:T(8,128)(2,1)S(1)} %bitcast.57, bf16[384,1024]{1,0:T(8,128)(2,1)S(1)} %copy-done.3), kind=kOutput, calls=%fused_computation.54 | convolution fusion | flops 1207959552 | bytes 22806528 | tf_op jit(solution)/shard_map/qhd,khd->hqk/dot_general | solution.py:155
  65.8 3.5 %convolution_convert_fusion.1 = bf16[1536,1024]{0,1:T(8,128)(2,1)} fusion(bf16[1536,512]{1,0:T(8,128)(2,1)S(1)} %constant_dynamic-update-slice_fusion, bf16[512,1024]{1,0:T(8,128)(2,1)S(1)} %copy-done.14), kind=kOutput, calls=%fused_computation.12 | convolution fusion | flops 1612185600 | bytes 5767168 | tf_op jit(solution)/shard_map/dot_general | solution.py:146
  69.2 12.9 %fusion.2 = f32[8,384,1536]{1,2,0:T(8,128)} fusion(f32[8,1536,384]{2,1,0:T(8,128)} %fusion.40, pred[384,1536]{0,1:T(8,128)(4,1)S(1)} %compare_and_fusion, bf16[384,8,32]{0,2,1:T(8,128)(2,1)S(1)} %get-tuple-element.16, bf16[384,8,32]{0,2,1:T(8,128)(2,1)S(1)} %get-tuple-element.15, bf16[384,32]{0,1:T(8,128)(2,1)S(1)} %get-tuple-element.18, ...), kind=kOutput, calls=%fused_computation.3 | convolution fusion | flops 619905024 | bytes 38928384 | tf_op jit(solution)/shard_map/qhr,kr->hqk/dot_general | solution.py:161
  82.1 15.3 %fusion.70 = f32[8,384]{1,0:T(8,128)S(1)} fusion(f32[8,384,1536]{1,2,0:T(8,128)} %fusion.2), kind=kOutput, calls=%fused_computation.125 | output fusion | flops 9438719 | bytes 18886656 | tf_op jit(solution)/shard_map/sub | solution.py:166
  97.5 17.5 %fusion.23 = bf16[8,128,384]{2,1,0:T(8,128)(2,1)S(1)} fusion(bf16[1536,8,128]{0,2,1:T(8,128)(2,1)} %bitcast.60, f32[8,384]{1,0:T(8,128)S(1)} %fusion.70, f32[8,384,1536]{1,2,0:T(8,128)} %fusion.2), kind=kOutput, calls=%fused_computation.32 | convolution fusion | flops 1222513152 | bytes 22818816 | tf_op jit(solution)/shard_map/hqk,khd->qhd/dot_general | solution.py:168
  115.0 4.0 %convolution_convert_fusion.3 = bf16[384,2048]{1,0:T(8,128)(2,1)S(1)} fusion(bf16[384,1024]{0,1:T(8,128)(2,1)S(1)} %bitcast.61, bf16[1024,2048]{1,0:T(8,128)(2,1)} %param.26), kind=kOutput, calls=%fused_computation.19 | convolution fusion | flops 1611399168 | bytes 6553600 | tf_op jit(solution)/shard_map/dot_general | solution.py:175
  119.2 23.5 %all_to_all.27 = bf16[4,384,512]{2,1,0:T(8,128)(2,1)S(1)} all-to-all(bf16[4,384,512]{2,1,0:T(8,128)(2,1)S(1)} %bitcast.54), channel_id=1, replica_groups=mesh['sp'=64,'tp'=4] {'tp'}, dimensions={0} | all-to-all | bytes 3145728 | tf_op jit(solution)/shard_map/all_to_all | solution.py:34
  142.7 0.2 convert_reduce_fusion.1
  142.9 0.2 fusion.46
  143.2 0.6 broadcast_in_dim.20
  143.8 3.2 %all-to-all-start.1 = ((f32[4,1,768]{2,1,0:T(1,128)}), f32[4,1,768]{2,1,0:T(1,128)S(1)}, u32[]{:S(2)}, u32[]{:S(2)}) async-start(f32[4,1,768]{2,1,0:T(1,128)} %broadcast_in_dim.20), calls=%async_computation.1 | async-start | bytes 24576 | tf_op jit(solution)/shard_map/all_to_all | solution.py:40
  147.1 5.3 %all-to-all-done.1 = f32[4,1,768]{2,1,0:T(1,128)S(1)} async-done(((f32[4,1,768]{2,1,0:T(1,128)}), f32[4,1,768]{2,1,0:T(1,128)S(1)}, u32[]{:S(2)}, u32[]{:S(2)}) %all-to-all-start.1) | async-done | bytes 12320 | tf_op jit(solution)/shard_map/all_to_all | solution.py:40
  152.4 0.2 add_convert_fusion.1
  152.9 1.3 broadcast_in_dim.21
  154.1 4.3 %all-to-all-start.2 = ((bf16[4,384,512]{1,2,0:T(8,128)(2,1)}), bf16[4,384,512]{1,2,0:T(8,128)(2,1)}, u32[]{:S(2)}, u32[]{:S(2)}) async-start(bf16[4,384,512]{1,2,0:T(8,128)(2,1)} %broadcast_in_dim.21), calls=%async_computation.2 | async-start | bytes 3145728 | tf_op jit(solution)/shard_map/all_to_all | solution.py:40
  158.6 3.5 %collective-permute-start.10 = (s32[2]{0:T(128)S(1)}, s32[2]{0:T(128)S(1)}, u32[]{:S(2)}, u32[]{:S(2)}) collective-permute-start(s32[2]{0:T(128)S(1)} %slice.78), channel_id=1, source_target_pairs={{0,4},{4,8},{8,12},{12,16},{16,20},{20,24},{24,28},{28,32},{32,36}... | collective-permute-start | bytes 32 | tf_op jit(solution)/shard_map/ppermute | solution.py:23
  162.2 1.2 collective-permute-done.10
  163.5 16.5 %all-to-all-done.2 = bf16[4,384,512]{1,2,0:T(8,128)(2,1)} async-done(((bf16[4,384,512]{1,2,0:T(8,128)(2,1)}), bf16[4,384,512]{1,2,0:T(8,128)(2,1)}, u32[]{:S(2)}, u32[]{:S(2)}) %all-to-all-start.2) | async-done | bytes 1572896 | tf_op jit(solution)/shard_map/all_to_all | solution.py:40
  180.0 5.9 %fusion.11 = bf16[384,1408]{1,0:T(8,128)(2,1)S(1)} fusion(bf16[384,2048]{0,1:T(8,128)(2,1)} %bitcast.10, bf16[2048,2816]{1,0:T(8,128)(2,1)} %all-gather.3.cloned.1.call-done), kind=kOutput, calls=%fused_computation.17 | convolution fusion | flops 2215133184 | bytes 8421376 | tf_op jit(solution)/shard_map/dot_general | solution.py:182
  185.9 2.4 collective-permute-start.11
  188.3 4.1 %fusion.8 = bf16[384,1408]{1,0:T(8,128)(2,1)S(1)} fusion(bf16[384,2048]{0,1:T(8,128)(2,1)} %bitcast.10, bf16[2048,2816]{1,0:T(8,128)(2,1)S(1)} %copy-done.13), kind=kOutput, calls=%fused_computation.16 | convolution fusion | flops 2215133184 | bytes 8421376 | tf_op jit(solution)/shard_map/dot_general | solution.py:183
  192.4 1.9 collective-permute-start.9
  194.4 2.9 %collective-permute-done.9 = bf16[2,1408]{1,0:T(2,128)(2,1)S(1)} collective-permute-done((bf16[2,1408]{1,0:T(2,128)(2,1)S(1)}, bf16[2,1408]{1,0:T(2,128)(2,1)S(1)}, u32[]{:S(2)}, u32[]{:S(2)}) %collective-permute-start.9) | collective-permute-done | bytes 5664 | tf_op jit(solution)/shard_map/ppermute | solution.py:23
  197.4 9.5 %convolution_convert_fusion.2 = bf16[384,2048]{1,0:T(8,128)(2,1)S(1)} fusion(bf16[1408,2048]{0,1:T(8,128)(2,1)} %all-gather.5.cloned.1.call-done, bf16[384,1408]{1,0:T(8,128)(2,1)S(1)} %fusion.11, bf16[384,1408]{1,0:T(8,128)(2,1)} %copy-done.12, bf16[2,1408]{1,0:T(2,128)(2,1)S(1)} %collective-permute-done.11, ...), kind=kOutput, calls=%fused_computation.18 | convolution fusion | flops 2239168512 | bytes 9552384 | tf_op jit(solution)/shard_map/dot_general | solution.py:218
  207.0 21.9 %all_to_all.28 = bf16[4,384,512]{2,1,0:T(8,128)(2,1)S(1)} all-to-all(bf16[4,384,512]{2,1,0:T(8,128)(2,1)S(1)} %bitcast.55), channel_id=1, replica_groups=mesh['sp'=64,'tp'=4] {'tp'}, dimensions={0} | all-to-all | bytes 3145728 | tf_op jit(solution)/shard_map/all_to_all | solution.py:34
  229.1 0.2 fusion.47
  229.4 0.6 broadcast_in_dim.22
  230.0 3.3 %all-to-all-start.4 = ((f32[4,1,768]{2,1,0:T(1,128)}), f32[4,1,768]{2,1,0:T(1,128)S(1)}, u32[]{:S(2)}, u32[]{:S(2)}) async-start(f32[4,1,768]{2,1,0:T(1,128)} %broadcast_in_dim.22), calls=%async_computation.4 | async-start | bytes 24576 | tf_op jit(solution)/shard_map/all_to_all | solution.py:40
  233.3 5.3 %all-to-all-done.4 = f32[4,1,768]{2,1,0:T(1,128)S(1)} async-done(((f32[4,1,768]{2,1,0:T(1,128)}), f32[4,1,768]{2,1,0:T(1,128)S(1)}, u32[]{:S(2)}, u32[]{:S(2)}) %all-to-all-start.4) | async-done | bytes 12320 | tf_op jit(solution)/shard_map/all_to_all | solution.py:40
  238.6 1.0 add_convert_fusion
  (76 shorter events, 1.6 us)
Async XLA Ops:
  6.5 49.0 %copy-start = (bf16[512,1024]{1,0:T(8,128)(2,1)S(1)}, bf16[512,1024]{1,0:T(8,128)(2,1)}, u32[]{:S(2)}) copy-start(bf16[512,1024]{1,0:T(8,128)(2,1)} %param.24) | copy-start | bytes 3145732
  6.5 31.1 %copy-start.5 = (s32[384]{0:T(512)S(1)}, s32[384]{0:T(512)}, u32[]{:S(2)}) copy-start(s32[384]{0:T(512)} %param.23) | copy-start | bytes 4612
  6.5 21.7 %copy-start.4 = (bf16[384,512]{1,0:T(8,128)(2,1)S(1)}, bf16[384,512]{1,0:T(8,128)(2,1)}, u32[]{:S(2)}) copy-start(bf16[384,512]{1,0:T(8,128)(2,1)} %param.21) | copy-start | bytes 1179652
  6.5 173.5 %all-gather.3.cloned.1.call-start = ((), (), s32[]{:S(2)}) async-start(), calls=%async_computation.5 | async-start | bytes 11714560 | tf_op jit(solution)/shard_map/all_gather | solution.py:70
  8.3 186.1 %all-gather.5.cloned.1.call-start = ((), (), s32[]{:S(2)}) async-start(), calls=%async_computation.6 | async-start | bytes 5857280 | tf_op jit(solution)/shard_map/all_gather | solution.py:220
  10.2 59.1 %collective-permute-start.6 = (bf16[384,64]{0,1:T(8,128)(2,1)S(1)}, bf16[384,64]{0,1:T(8,128)(2,1)S(1)}, u32[]{:S(2)}, u32[]{:S(2)}) collective-permute-start(bf16[384,64]{0,1:T(8,128)(2,1)S(1)} %pad_maximum_fusion.3), channel_id=1, source_target_pairs={{0,12},{4,16},{8,20},{12,24},{16,28},{20,32},{24,36},{28,40},{32,4... | collective-permute-start | bytes 147464 | tf_op jit(solution)/shard_map/ppermute | solution.py:23
  13.4 55.9 %collective-permute-start.7 = (bf16[384,64]{0,1:T(8,128)(2,1)S(1)}, bf16[384,64]{0,1:T(8,128)(2,1)S(1)}, u32[]{:S(2)}, u32[]{:S(2)}) collective-permute-start(bf16[384,64]{0,1:T(8,128)(2,1)S(1)} %pad_maximum_fusion.3), channel_id=1, source_target_pairs={{0,8},{4,12},{8,16},{12,20},{16,24},{20,28},{24,32},{28,36},{32,40... | collective-permute-start | bytes 147464 | tf_op jit(solution)/shard_map/ppermute | solution.py:23
  16.8 11.5 %collective-permute-start.3 = (s32[384]{0:T(512)}, s32[384]{0:T(512)S(1)}, u32[]{:S(2)}, u32[]{:S(2)}) collective-permute-start(s32[384]{0:T(512)} %param.23), channel_id=1, source_target_pairs={{0,12},{4,16},{8,20},{12,24},{16,28},{20,32},{24,36},{28,40},{32,4... | collective-permute-start | bytes 4616 | tf_op jit(solution)/shard_map/ppermute | solution.py:23
  20.8 12.2 %collective-permute-start.4 = (s32[384]{0:T(512)}, s32[384]{0:T(512)S(1)}, u32[]{:S(2)}, u32[]{:S(2)}) collective-permute-start(s32[384]{0:T(512)} %param.23), channel_id=1, source_target_pairs={{0,8},{4,12},{8,16},{12,20},{16,24},{20,28},{24,32},{28,36},{32,40... | collective-permute-start | bytes 4616 | tf_op jit(solution)/shard_map/ppermute | solution.py:23
  24.0 11.6 %collective-permute-start.5 = (s32[384]{0:T(512)}, s32[384]{0:T(512)S(1)}, u32[]{:S(2)}, u32[]{:S(2)}) collective-permute-start(s32[384]{0:T(512)} %param.23), channel_id=1, source_target_pairs={{0,4},{4,8},{8,12},{12,16},{16,20},{20,24},{24,28},{28,32},{32,36}... | collective-permute-start | bytes 4616 | tf_op jit(solution)/shard_map/ppermute | solution.py:23
  28.3 17.9 %collective-permute-start = (bf16[384,512]{1,0:T(8,128)(2,1)S(1)}, bf16[384,512]{1,0:T(8,128)(2,1)S(1)}, u32[]{:S(2)}, u32[]{:S(2)}) collective-permute-start(bf16[384,512]{1,0:T(8,128)(2,1)S(1)} %copy-done.4), channel_id=1, source_target_pairs={{0,12},{4,16},{8,20},{12,24},{16,28},{20,32},{24,36},{28,40},{32,4... | collective-permute-start | bytes 1179656 | tf_op jit(solution)/shard_map/ppermute | solution.py:23
  33.1 22.4 %collective-permute-start.1 = (bf16[384,512]{1,0:T(8,128)(2,1)S(1)}, bf16[384,512]{1,0:T(8,128)(2,1)S(1)}, u32[]{:S(2)}, u32[]{:S(2)}) collective-permute-start(bf16[384,512]{1,0:T(8,128)(2,1)S(1)} %copy-done.4), channel_id=1, source_target_pairs={{0,8},{4,12},{8,16},{12,20},{16,24},{20,28},{24,32},{28,36},{32,40... | collective-permute-start | bytes 1179656 | tf_op jit(solution)/shard_map/ppermute | solution.py:23
  35.6 19.9 %collective-permute-start.2 = (bf16[384,512]{1,0:T(8,128)(2,1)S(1)}, bf16[384,512]{1,0:T(8,128)(2,1)S(1)}, u32[]{:S(2)}, u32[]{:S(2)}) collective-permute-start(bf16[384,512]{1,0:T(8,128)(2,1)S(1)} %copy-done.4), channel_id=1, source_target_pairs={{0,4},{4,8},{8,12},{12,16},{16,20},{20,24},{24,28},{28,32},{32,36}... | collective-permute-start | bytes 1179656 | tf_op jit(solution)/shard_map/ppermute | solution.py:23
  46.1 23.1 %collective-permute-start.8 = (bf16[384,64]{0,1:T(8,128)(2,1)S(1)}, bf16[384,64]{0,1:T(8,128)(2,1)S(1)}, u32[]{:S(2)}, u32[]{:S(2)}) collective-permute-start(bf16[384,64]{0,1:T(8,128)(2,1)S(1)} %pad_maximum_fusion.3), channel_id=1, source_target_pairs={{0,4},{4,8},{8,12},{12,16},{16,20},{20,24},{24,28},{28,32},{32,36}... | collective-permute-start | bytes 147464 | tf_op jit(solution)/shard_map/ppermute | solution.py:23
  55.6 1.9 copy-start.3
  57.4 8.3 %copy-start.14 = (bf16[512,1024]{1,0:T(8,128)(2,1)S(1)}, bf16[512,1024]{1,0:T(8,128)(2,1)}, u32[]{:S(2)}) copy-start(bf16[512,1024]{1,0:T(8,128)(2,1)} %param.25) | copy-start | bytes 3145732
  119.1 23.7 %copy-start.2 = (bf16[384,512]{1,0:T(8,128)(2,1)S(1)}, bf16[384,512]{1,0:T(8,128)(2,1)}, u32[]{:S(2)}) copy-start(bf16[384,512]{1,0:T(8,128)(2,1)} %param.18) | copy-start | bytes 1179652
  142.7 4.4 %copy-start.8 = (bf16[512]{0:T(512)(128)(2,1)S(1)}, bf16[512]{0:T(512)(128)(2,1)}, u32[]{:S(2)}) copy-start(bf16[512]{0:T(512)(128)(2,1)} %param.27) | copy-start | bytes 3076
  142.7 4.4 %copy-start.9 = (bf16[512]{0:T(512)(128)(2,1)S(1)}, bf16[512]{0:T(512)(128)(2,1)}, u32[]{:S(2)}) copy-start(bf16[512]{0:T(512)(128)(2,1)} %param.28) | copy-start | bytes 3076
  143.8 8.6 %all-to-all-start.1 = ((f32[4,1,768]{2,1,0:T(1,128)}), f32[4,1,768]{2,1,0:T(1,128)S(1)}, u32[]{:S(2)}, u32[]{:S(2)}) async-start(f32[4,1,768]{2,1,0:T(1,128)} %broadcast_in_dim.20), calls=%async_computation.1 | async-start | bytes 24576 | tf_op jit(solution)/shard_map/all_to_all | solution.py:40
  152.8 9.3 %copy-start.6 = (bf16[3,1408]{1,0:T(4,128)(2,1)S(1)}, bf16[3,1408]{1,0:T(4,128)(2,1)}, u32[]{:S(2)}) copy-start(bf16[3,1408]{1,0:T(4,128)(2,1)} %param.31) | copy-start | bytes 25348
  152.8 9.3 %copy-start.7 = (bf16[3,1408]{1,0:T(4,128)(2,1)S(1)}, bf16[3,1408]{1,0:T(4,128)(2,1)}, u32[]{:S(2)}) copy-start(bf16[3,1408]{1,0:T(4,128)(2,1)} %param.32) | copy-start | bytes 25348
  154.1 25.9 %all-to-all-start.2 = ((bf16[4,384,512]{1,2,0:T(8,128)(2,1)}), bf16[4,384,512]{1,2,0:T(8,128)(2,1)}, u32[]{:S(2)}, u32[]{:S(2)}) async-start(bf16[4,384,512]{1,2,0:T(8,128)(2,1)} %broadcast_in_dim.21), calls=%async_computation.2 | async-start | bytes 3145728 | tf_op jit(solution)/shard_map/all_to_all | solution.py:40
  158.6 4.9 %collective-permute-start.10 = (s32[2]{0:T(128)S(1)}, s32[2]{0:T(128)S(1)}, u32[]{:S(2)}, u32[]{:S(2)}) collective-permute-start(s32[2]{0:T(128)S(1)} %slice.78), channel_id=1, source_target_pairs={{0,4},{4,8},{8,12},{12,16},{16,20},{20,24},{24,28},{28,32},{32,36}... | collective-permute-start | bytes 32 | tf_op jit(solution)/shard_map/ppermute | solution.py:23
  180.0 8.3 %copy-start.13 = (bf16[2048,2816]{1,0:T(8,128)(2,1)S(1)}, bf16[2048,2816]{1,0:T(8,128)(2,1)}, u32[]{:S(2)}) copy-start(bf16[2048,2816]{1,0:T(8,128)(2,1)} %all-gather.3.cloned.1.call-done) | copy-start | bytes 34603012
  185.9 8.5 %collective-permute-start.11 = (bf16[2,1408]{1,0:T(2,128)(2,1)S(1)}, bf16[2,1408]{1,0:T(2,128)(2,1)S(1)}, u32[]{:S(2)}, u32[]{:S(2)}) collective-permute-start(bf16[2,1408]{1,0:T(2,128)(2,1)S(1)} %slice.99), channel_id=1, source_target_pairs={{0,4},{4,8},{8,12},{12,16},{16,20},{20,24},{24,28},{28,32},{32,36}... | collective-permute-start | bytes 16904 | tf_op jit(solution)/shard_map/ppermute | solution.py:23
  192.4 2.0 copy-start.12
  192.4 4.9 %collective-permute-start.9 = (bf16[2,1408]{1,0:T(2,128)(2,1)S(1)}, bf16[2,1408]{1,0:T(2,128)(2,1)S(1)}, u32[]{:S(2)}, u32[]{:S(2)}) collective-permute-start(bf16[2,1408]{1,0:T(2,128)(2,1)S(1)} %slice.96), channel_id=1, source_target_pairs={{0,4},{4,8},{8,12},{12,16},{16,20},{20,24},{24,28},{28,32},{32,36}... | collective-permute-start | bytes 16904 | tf_op jit(solution)/shard_map/ppermute | solution.py:23
  207.0 32.6 %copy-start.1 = (bf16[512,1024]{1,0:T(8,128)(2,1)S(1)}, bf16[512,1024]{1,0:T(8,128)(2,1)}, u32[]{:S(2)}) copy-start(bf16[512,1024]{1,0:T(8,128)(2,1)} %param.24) | copy-start | bytes 3145732
  228.9 4.4 %copy-start.10 = (bf16[512]{0:T(512)(128)(2,1)S(1)}, bf16[512]{0:T(512)(128)(2,1)}, u32[]{:S(2)}) copy-start(bf16[512]{0:T(512)(128)(2,1)} %param.34) | copy-start | bytes 3076
  228.9 4.4 %copy-start.11 = (bf16[512]{0:T(512)(128)(2,1)S(1)}, bf16[512]{0:T(512)(128)(2,1)}, u32[]{:S(2)}) copy-start(bf16[512]{0:T(512)(128)(2,1)} %param.35) | copy-start | bytes 3076
  230.0 8.6 %all-to-all-start.4 = ((f32[4,1,768]{2,1,0:T(1,128)}), f32[4,1,768]{2,1,0:T(1,128)S(1)}, u32[]{:S(2)}, u32[]{:S(2)}) async-start(f32[4,1,768]{2,1,0:T(1,128)} %broadcast_in_dim.22), calls=%async_computation.4 | async-start | bytes 24576 | tf_op jit(solution)/shard_map/all_to_all | solution.py:40
Sparse Core Ops, SparseCore 0:
  10.1 88.8 all-gather.2
  101.7 77.0 all-gather.4
where the time goes:
time: 250 us; the launch traced here: 246 us
  matrix products  67.5 us (27%)
  starting transfers between devices  46.7 us (19%)
  waiting for transfers between devices  46.2 us (18%)
  blocking collectives  45.4 us (18%)
  other arithmetic  22.2 us (9%)
  between operations  14 us (6%)
  local copies, waits for them, and re-layouts  4.4 us (2%)
    all_to_all x2, blocking collectives, sum_at_owner(): lax.all_to_all(parts, axis, split_axis=0, concat_axis=0, tiled=True)  45.4 us
    ppermute x12, starting transfers between devices, passed_along(): return lax.ppermute(value, axis, pairs)  35.8 us
    all_to_all x3, waiting for transfers between devices, from_everyone(): return lax.all_to_all(copies, axis, split_axis=0, concat_axis=0, tiled=True)  27 us
    ppermute x12, waiting for transfers between devices, passed_along(): return lax.ppermute(value, axis, pairs)  18.5 us
    dot_general x1, matrix products, local(): jnp.einsum('hqk,khd->qhd', weights, values.reshape(window, head_count, VD...  17.5 us
    sub x1, other arithmetic, local(): weights = jnp.exp(scores - row_max)  15.3 us
    dot_general x1, matrix products, local(): jnp.einsum('qhr,kr->hqk', turned_query, win_key, preferred_element_type=j...  12.9 us
    all_to_all x3, starting transfers between devices, from_everyone(): return lax.all_to_all(copies, axis, split_axis=0, concat_axis=0, tiled=True)  10.8 us
  transfers between devices with their start and end apart: 17, of which 7 were waited for; matrix products, arithmetic and copies ran while one was open for 33% of the time, Pallas kernels for 0%

commit v1 on v0

v1 whole, which is shorter than its diff:
```python
import jax
import jax.numpy as jnp
from jax import lax
from jax.experimental import pallas as pl
from jax.experimental.pallas import tpu as pltpu
from jax.sharding import PartitionSpec as P

D = 2048
NOPE = 128
ROPE = 64
VDIM = 128
CONV = 3
REACH = 3

norm_eps = 1e-05
residual_scale = 8.0**0.25
rope_base_freq = 10000.0
masked_score = -1e30
SCALE2 = (NOPE + ROPE) ** (-0.5) * 1.4426950408889634

NX, NZ, NY = 4, 8, 4
ROWS = 384
HALF = ROWS // 2
CH = 512
UNITS = 1408
DA = 512
LA = DA + UNITS
LW = 3 * UNITS
PACKW = 640
PACKR = 400
MESH = pl.DeviceIdType.MESH
BF = jnp.bfloat16
F32 = jnp.float32


def dot(a, b):
    return jnp.dot(a, b, preferred_element_type=F32)


def dot_nt(a, b):
    return lax.dot_general(a, b, (((1,), (1,)), ((), ())), preferred_element_type=F32)


def layer_kernel(
    pack_h, qn_h, qr_h, kup_h, vup_h, op_h, res_h, wsh_h, gb_ref, cv_ref,
    out_ref,
    packs, qn, qr, kup, vup, op, res, w, gbs, att, acc, mrun, lrun, dcol,
    sa, sp_buf, sm_buf, pfp, pfm, own, ra, rb, ra2, rb2, m4, nf, gv, hid, stat, stats,
    lsem, ssem, rsem,
):
    sp = lax.axis_index("sp")
    y = lax.axis_index("tp")
    c = lax.rem(sp, 2)
    k = lax.div(sp, 2)
    x = lax.rem(k, NX)
    z = lax.div(k, NX)

    def wrap(v, n):
        return lax.rem(v + n, n)

    def dev(zz, xx, cc, yy):
        return ((wrap(zz, NZ) * NX + wrap(xx, NX)) * 2 + cc, wrap(yy, NY))

    def chip(kk, cc):
        return (wrap(kk, NZ * NX) * 2 + cc, y)

    xp, xm = dev(z, x + 1, c, y), dev(z, x - 1, c, y)
    zp, zm = dev(z + 1, x, c, y), dev(z - 1, x, c, y)
    sib = dev(z, x, 1 - c, y)
    yp, ym, yy = dev(z, x, c, y + 1), dev(z, x, c, y - 1), dev(z, x, c, y + 2)
    nextc, prevc = chip(k + 1, c), chip(k - 1, c)
    nexto, prevo = chip(k + 1, 1 - c), chip(k - 1, 1 - c)

    local = []
    def fetch(src, dst):
        d = pltpu.make_async_copy(src, dst, lsem.at[len(local)])
        d.start()
        local.append(d)
        return d
    f_pack = fetch(pack_h, packs.at[0])
    f_w = fetch(wsh_h, w.at[z, x, c])
    f_kup = fetch(kup_h, kup)
    f_qn = fetch(qn_h, qn)
    f_qr = fetch(qr_h, qr)
    f_vup = fetch(vup_h, vup)
    f_op = fetch(op_h, op)
    f_res = fetch(res_h, res)

    barrier = pltpu.get_barrier_semaphore()
    peers = (xp, xm, zp, zm, sib, yp, ym, yy, nextc, prevc, nexto, prevo)
    for p in peers:
        pl.semaphore_signal(barrier, inc=1, device_id=p, device_id_type=MESH)
    pl.semaphore_wait(barrier, len(peers))

    sends = []
    names = {}

    def rid(name):
        return names.setdefault(name, len(names))

    def copy_to(src, dst, to, name):
        d = pltpu.make_async_remote_copy(
            src_ref=src, dst_ref=dst, send_sem=ssem.at[len(sends)],
            recv_sem=rsem.at[rid(name)], device_id=to, device_id_type=MESH,
        )
        sends.append(d)
        return d

    def send(src, dst, to, name):
        copy_to(src, dst, to, name).start()

    def arrive(dst, name):
        pltpu.make_async_remote_copy(
            src_ref=dst, dst_ref=dst, send_sem=ssem.at[0],
            recv_sem=rsem.at[rid(name)], device_id=sib, device_id_type=MESH,
        ).wait_recv()

    def wa(dz, dx):
        return w.at[wrap(z + dz, NZ), wrap(x + dx, NX), c, :, pl.ds(0, LA)]

    def za(dz, cc, lo=0, n=NX):
        return w.at[wrap(z + dz, NZ), pl.ds(lo, n), cc, :, pl.ds(0, LA)]

    def wb(dz, lo=LA, n=LW - LA):
        return w.at[wrap(z + dz, NZ), x, c, :, pl.ds(lo, n)]

    def xb(dx, cc, lo=0, n=NZ):
        return w.at[pl.ds(lo, n), wrap(x + dx, NX), cc, :, pl.ds(LA, LW - LA)]

    BH = (LW - LA) // 2
    HZ = NZ // 2
    HX = NX // 2

    def same(ref, to, name):
        send(ref, ref, to, name)

    def a_start():
        same(wa(0, 0), xp, "a1m")
        same(wa(0, 0), xm, "a1p")

    def a_one():
        arrive(wa(0, 1), "a1p")
        same(wa(0, 1), xm, "a2p")

    def a_two():
        arrive(wa(0, -1), "a1m")
        arrive(wa(0, 2), "a2p")
        same(za(0, c), zp, "z1m")
        same(za(0, c), zm, "z1p")
        same(za(0, c), sib, "sz0")

    def a_step(s):
        arrive(za(-s, c), f"z{s}m")
        arrive(za(s, c), f"z{s}p")
        if s < 3:
            same(za(-s, c), zp, f"z{s + 1}m")
            same(za(s, c), zm, f"z{s + 1}p")
        else:
            same(za(-s, c, 0, HX), zp, "z4m")
            same(za(s, c, HX, HX), zm, "z4p")
        same(za(-s, c), sib, f"sz{s}m")
        same(za(s, c), sib, f"sz{s}p")

    def a_last():
        arrive(za(4, c, 0, HX), "z4m")
        arrive(za(4, c, HX, HX), "z4p")
        same(za(4, c), sib, "sz4")

    def a_done():
        arrive(za(0, 1 - c), "sz0")
        for s in (1, 2, 3):
            arrive(za(-s, 1 - c), f"sz{s}m")
            arrive(za(s, 1 - c), f"sz{s}p")
        arrive(za(4, 1 - c), "sz4")

    def b_start():
        same(wb(0), zp, "b1m")
        same(wb(0), zm, "b1p")

    def b_step(s):
        arrive(wb(-s), f"b{s}m")
        arrive(wb(s), f"b{s}p")
        if s < 3:
            same(wb(-s), zp, f"b{s + 1}m")
            same(wb(s), zm, f"b{s + 1}p")
        else:
            same(wb(-s, LA, BH), zp, "b4m")
            same(wb(s, LA + BH, BH), zm, "b4p")

    def b_turn():
        arrive(wb(4, LA, BH), "b4m")
        arrive(wb(4, LA + BH, BH), "b4p")
        same(xb(0, c), xp, "x1m")
        same(xb(0, c), xm, "x1p")
        same(xb(0, c), sib, "sx0")

    def b_cross():
        arrive(xb(-1, c), "x1m")
        arrive(xb(1, c), "x1p")
        same(xb(-1, c, 0, HZ), xp, "x2m")
        same(xb(1, c, HZ, HZ), xm, "x2p")
        same(xb(-1, c), sib, "sx1m")
        same(xb(1, c), sib, "sx1p")

    def b_last():
        arrive(xb(2, c, 0, HZ), "x2m")
        arrive(xb(2, c, HZ, HZ), "x2p")
        same(xb(2, c), sib, "sx2")

    def b_done():
        arrive(xb(0, 1 - c), "sx0")
        arrive(xb(-1, 1 - c), "sx1m")
        arrive(xb(1, 1 - c), "sx1p")
        arrive(xb(2, 1 - c), "sx2")

    f_w.wait()
    a_start()
    b_start()
    f_pack.wait()
    third_at = len(sends)
    third = copy_to(packs.at[0], packs.at[1], sib, "l1")

    @pl.when(c == 0)
    def _():
        third.start()

    send(packs.at[0], packs.at[2], nextc, "l2")
    send(gb_ref, gbs.at[y], yp, "gm")
    send(gb_ref, gbs.at[y], ym, "gp")
    send(gb_ref, gbs.at[y], yy, "g2")

    def doc_column(slot):
        return packs[slot, 0:ROWS, 512:640].astype(F32)[:, ROPE : ROPE + 1]

    dcol[8 : 8 + ROWS, :] = jnp.broadcast_to(doc_column(0), (ROWS, 128))

    def attend(slot, back, kind, first=False, last=False):
        exists = sp >= back

        def body(pair, carry):
            off = pl.multiple_of(pair * 256, 256)
            lat = packs[slot, 0:ROWS, 0:512]
            kr = packs[slot, 0:ROWS, 512:640]
            kdoc = packs[slot, ROWS:PACKR, 0:ROWS].astype(F32)[0:1, :]
            kdoc = jnp.where(exists, kdoc, -1.0)
            k2 = dot(lat, kup[:, pl.ds(off, 256)]).astype(BF)
            v2 = dot(lat, vup[:, pl.ds(off, 256)]).astype(BF)
            for hh in range(2):
                h = pair * 2 + hh
                lanes = pl.ds(pl.multiple_of(off + hh * 128, 128), 128)
                kk = jnp.concatenate([k2[:, hh * 128 : hh * 128 + 128], kr], axis=1)
                vv = v2[:, hh * 128 : hh * 128 + 128]
                for qi in range(3):
                    r0 = qi * 128
                    rows = pl.ds(r0, 128)
                    lo, hi = 0, ROWS
                    if kind == "diag":
                        hi = r0 + 128
                    if kind == "far":
                        lo = r0
                    q = jnp.concatenate([qn[rows, lanes], qr[rows, lanes]], axis=1)
                    s = dot_nt(q, kk[lo:hi])
                    qdoc = dcol[8 + r0 : 8 + r0 + 128, 0:1]
                    ok = qdoc == kdoc[:, lo:hi]
                    if kind == "diag":
                        qi_pos = lax.broadcasted_iota(jnp.int32, s.shape, 0) + r0
                        ki_pos = lax.broadcasted_iota(jnp.int32, s.shape, 1)
                        ok = ok & (ki_pos <= qi_pos)
                    s = jnp.where(ok, s, masked_score)
                    mx = jnp.max(s, axis=1, keepdims=True)
                    if first:
                        p = jnp.exp2((s - mx) * SCALE2)
                        total = jnp.broadcast_to(jnp.sum(p, axis=1, keepdims=True), (128, 128))
                        o = dot(p.astype(BF), vv[lo:hi])
                        mnew = jnp.broadcast_to(mx, (128, 128))
                    else:
                        mold = mrun[h, rows, :]
                        mnew = jnp.maximum(mold, mx)
                        alpha = jnp.exp2((mold - mnew) * SCALE2)
                        p = jnp.exp2((s - mnew[:, 0:1]) * SCALE2)
                        total = lrun[h, rows, :] * alpha + jnp.sum(p, axis=1, keepdims=True)
                        o = acc[h, rows, :] * alpha + dot(p.astype(BF), vv[lo:hi])
                    if last:
                        att[rows, lanes] = (o / total).astype(BF)
                    else:
                        mrun[h, rows, :] = mnew
                        lrun[h, rows, :] = total
                        acc[h, rows, :] = o
            return carry

        lax.fori_loop(0, 4, body, 0)

    f_kup.wait()
    f_qn.wait()
    f_qr.wait()
    f_vup.wait()
    attend(0, 0, "diag", first=True)
    a_one()
    b_step(1)
    a_two()
    b_step(2)
    b_step(3)
    arrive(packs.at[2], "l2")
    hand = copy_to(packs.at[2], packs.at[3 - 2 * c], sib, "l1")
    hand_three = pltpu.make_async_remote_copy(
        src_ref=packs.at[2], dst_ref=packs.at[3], send_sem=ssem.at[len(sends) - 1],
        recv_sem=rsem.at[rid("l3")], device_id=sib, device_id_type=MESH,
    )
    relay = pltpu.make_async_remote_copy(
        src_ref=packs.at[2], dst_ref=packs.at[3], send_sem=ssem.at[third_at],
        recv_sem=rsem.at[rid("l3")], device_id=nexto, device_id_type=MESH,
    )
    hand_one = pltpu.make_async_remote_copy(
        src_ref=packs.at[2], dst_ref=packs.at[1], send_sem=ssem.at[len(sends) - 1],
        recv_sem=rsem.at[rid("l1")], device_id=sib, device_id_type=MESH,
    )

    @pl.when(c == 0)
    def _():
        hand_three.start()

    @pl.when(c == 1)
    def _():
        hand_one.start()
        relay.start()

    attend(2, 2, "full")
    b_turn()
    arrive(packs.at[1], "l1")
    before = jnp.where(sp >= 1, doc_column(1)[ROWS - 8 : ROWS, :], -1.0)
    dcol[0:8, :] = jnp.broadcast_to(before, (8, 128))
    attend(1, 1, "full")
    arrive(packs.at[3], "l3")
    attend(3, 3, "far", last=True)
    a_step(1)

    def shared_sum(chunk, tag, ra, rb, pump_one, pump_two):
        f = chunk(wrap(y + 2, NY))
        sa[...] = f.astype(BF)
        send(sa.at[pl.ds(0, HALF)], ra.at[0], yp, tag + "am")
        send(sa.at[pl.ds(HALF, HALF)], ra.at[1], ym, tag + "ap")
        f = chunk(wrap(y + 1, NY))
        pfp[...] = f[:HALF]
        sp_buf[pl.ds(HALF, HALF), :] = f[HALF:].astype(BF)
        send(sp_buf.at[pl.ds(HALF, HALF)], rb.at[0, pl.ds(HALF, HALF)], yp, tag + "bm1")
        f = chunk(wrap(y - 1, NY))
        pfm[...] = f[HALF:]
        sm_buf[pl.ds(0, HALF), :] = f[:HALF].astype(BF)
        send(sm_buf.at[pl.ds(0, HALF)], rb.at[1, pl.ds(0, HALF)], ym, tag + "bp0")
        own[...] = chunk(y)
        pump_one()
        arrive(ra.at[0], tag + "am")
        sp_buf[pl.ds(0, HALF), :] = (pfp[...] + ra[0].astype(F32)).astype(BF)
        send(sp_buf.at[pl.ds(0, HALF)], rb.at[0, pl.ds(0, HALF)], yp, tag + "bm0")
        arrive(ra.at[1], tag + "ap")
        sm_buf[pl.ds(HALF, HALF), :] = (pfm[...] + ra[1].astype(F32)).astype(BF)
        send(sm_buf.at[pl.ds(HALF, HALF)], rb.at[1, pl.ds(HALF, HALF)], ym, tag + "bp1")
        pump_two()
        arrive(rb.at[0, pl.ds(HALF, HALF)], tag + "bm1")
        arrive(rb.at[1, pl.ds(0, HALF)], tag + "bp0")
        arrive(rb.at[0, pl.ds(0, HALF)], tag + "bm0")
        arrive(rb.at[1, pl.ds(HALF, HALF)], tag + "bp1")
        return own[...] + rb[0].astype(F32) + rb[1].astype(F32)

    def settle(ds):
        for d in ds:
            d.wait_send()

    f_op.wait()
    f_res.wait()

    def head_share(t):
        return dot(att[...], op[:, pl.ds(pl.multiple_of(t * CH, CH), CH)])

    mark = len(sends)
    total_one = shared_sum(head_share, "p", ra, rb, lambda: None, lambda: a_step(2))
    m4[y] = (residual_scale * res[...].astype(F32) + total_one).astype(BF)

    def piece(dy, lo):
        return m4.at[wrap(y + dy, NY), pl.ds(lo, HALF)]

    same(piece(0, 0), yp, "m1m0")
    same(piece(0, HALF), ym, "m1p1")
    same(piece(0, HALF), yp, "m1m1")
    same(piece(0, 0), ym, "m1p0")
    b_cross()
    arrive(piece(-1, 0), "m1m0")
    same(piece(-1, 0), yp, "m2m")
    arrive(piece(1, HALF), "m1p1")
    same(piece(1, HALF), ym, "m2p")
    arrive(gbs.at[wrap(y - 1, NY)], "gm")
    arrive(gbs.at[wrap(y + 1, NY)], "gp")
    arrive(gbs.at[wrap(y + 2, NY)], "g2")
    gbs[y] = gb_ref[...]
    a_step(3)
    arrive(piece(-1, HALF), "m1m1")
    arrive(piece(1, 0), "m1p0")
    arrive(piece(2, 0), "m2m")
    arrive(piece(2, HALF), "m2p")

    def norm_rows(i, carry):
        rows = pl.ds(pl.multiple_of(i * 32, 32), 32)
        parts = [m4[t, rows, :].astype(F32) for t in range(NY)]
        s = sum(jnp.sum(v, axis=1, keepdims=True) for v in parts) / D
        q = sum(jnp.sum(v * v, axis=1, keepdims=True) for v in parts) / D
        r = lax.rsqrt(q - s * s + norm_eps)
        for t in range(NY):
            nf[rows, t * CH : (t + 1) * CH] = (
                (parts[t] - s) * r * gbs[t, 0:1, :] + gbs[t, 1:2, :]
            ).astype(BF)
        return carry

    lax.fori_loop(0, ROWS // 32, norm_rows, 0)
    b_last()
    a_last()
    b_done()
    a_done()

    def up(j, carry):
        lanes = pl.ds(pl.multiple_of(DA + j * 256, 128), 256)
        f = dot(nf[...], w[:, :, :, :, lanes].reshape(D, 256))
        gv[8 : 8 + ROWS, pl.ds(pl.multiple_of(j * 256, 256), 256)] = f
        return carry

    lax.fori_loop(0, 2 * UNITS // 256, up, 0)
    tail = pl.ds(ROWS, 8)

    to_sib = copy_to(gv.at[tail], stat.at[0], sib, "t")
    to_next = pltpu.make_async_remote_copy(
        src_ref=gv.at[tail], dst_ref=stat.at[0], send_sem=ssem.at[len(sends) - 1],
        recv_sem=rsem.at[rid("t")], device_id=nexto, device_id_type=MESH,
    )

    @pl.when(c == 0)
    def _():
        to_sib.start()

    @pl.when(c == 1)
    def _():
        to_next.start()

    def conv_block(r0):
        here = dcol[8 + r0 : 8 + r0 + 128, :]
        one = (dcol[7 + r0 : 7 + r0 + 128, :] == here).astype(F32)
        two = (dcol[6 + r0 : 6 + r0 + 128, :] == here).astype(F32)

        def cols(j, carry):
            def mix(base):
                lanes = pl.ds(pl.multiple_of(base + j * 128, 128), 128)
                a0 = gv[6 + r0 : 6 + r0 + 128, lanes]
                a1 = gv[7 + r0 : 7 + r0 + 128, lanes]
                a2 = gv[8 + r0 : 8 + r0 + 128, lanes]
                return (
                    cv_ref[0:1, lanes] * a0 * two
                    + cv_ref[1:2, lanes] * a1 * one
                    + cv_ref[2:3, lanes] * a2
                )

            g = mix(0)
            v = mix(UNITS)
            act = 0.5 * g * (1.0 + jnp.tanh(0.7978845608028654 * (g + 0.044715 * (g * g * g))))
            hid[r0 : r0 + 128, pl.ds(pl.multiple_of(j * 128, 128), 128)] = (v * act).astype(BF)
            return carry

        lax.fori_loop(0, UNITS // 128, cols, 0)

    conv_block(256)
    conv_block(128)
    arrive(stat.at[0], "t")
    gv[0:8, :] = jnp.where(sp >= 1, stat[0], 0.0)
    conv_block(0)

    def unit_share(t):
        rows = pl.ds(2 * t, 2)
        da = w[rows, :, :, :, 0:DA].reshape(CH, DA)
        db = w[rows, :, :, :, LA + UNITS : LW].reshape(CH, UNITS - DA)
        return dot_nt(hid[:, 0:DA], da) + dot_nt(hid[:, DA:UNITS], db)

    settle(sends[mark : mark + 6])
    total_two = shared_sum(unit_share, "u", ra2, rb2, lambda: None, lambda: None)
    mixed = (
        residual_scale * nf[:, pl.ds(pl.multiple_of(y * CH, CH), CH)].astype(F32) + total_two
    )
    own[...] = mixed
    lane = lax.broadcasted_iota(jnp.int32, (ROWS, 128), 1)
    s = jnp.sum(mixed, axis=1, keepdims=True)
    q = jnp.sum(mixed * mixed, axis=1, keepdims=True)
    both = jnp.where(lane == 0, s, jnp.where(lane == 1, q, 0.0))
    stats[y] = both.T[0:8, :]
    same(stats.at[y], yp, "qm")
    same(stats.at[y], ym, "qp")
    same(stats.at[y], yy, "q2")
    arrive(stats.at[wrap(y - 1, NY)], "qm")
    arrive(stats.at[wrap(y + 1, NY)], "qp")
    arrive(stats.at[wrap(y + 2, NY)], "q2")
    tot = (stats[0] + stats[1]) + (stats[2] + stats[3])
    back = jnp.concatenate([tot, jnp.zeros((120, ROWS), F32)], axis=0).T
    s = back[:, 0:1] / D
    q = back[:, 1:2] / D
    r = lax.rsqrt(q - s * s + norm_eps)
    out_ref[...] = ((own[...] - s) * r * gb_ref[2:3, :] + gb_ref[3:4, :]).astype(BF)
    settle(sends[:mark])
    settle(sends[mark + 6 :])


N_SEND = 72
N_RECV = 72


def tables(positions):
    frequencies = 1.0 / rope_base_freq ** (jnp.arange(0, ROPE, 2, dtype=jnp.float32) / ROPE)
    angles = positions.astype(jnp.float32)[:, None] * frequencies[None, :]
    return (jnp.cos(angles), jnp.sin(angles))


def rotate(vectors, cosine, sine_table):
    half_width = vectors.shape[-1] // 2
    front_half = vectors[..., :half_width]
    back_half = vectors[..., half_width:]
    return jnp.concatenate(
        [
            front_half * cosine - back_half * sine_table,
            front_half * sine_table + back_half * cosine,
        ],
        axis=-1,
    )


def local(
    residual, query_nope, query_rope, latent, rope_key, doc_ids, key_up, value_up, out_proj,
    norm1_gain, norm1_bias, ffn_gate, ffn_value, conv_gate, conv_value, ffn_down,
    norm2_gain, norm2_bias,
):
    rows = latent.shape[0]
    heads = query_nope.shape[1] // NOPE
    positions = lax.axis_index("sp") * rows + jnp.arange(rows, dtype=jnp.int32)
    cosine, sine = tables(positions)
    turned_key = rotate(rope_key.astype(F32), cosine, sine).astype(BF)
    turned_query = rotate(
        query_rope.astype(F32).reshape(rows, heads, ROPE), cosine[:, None], sine[:, None]
    ).astype(BF)
    turned_query = jnp.pad(turned_query, ((0, 0), (0, 0), (0, 128 - ROPE))).reshape(rows, heads * 128)
    doc = doc_ids.astype(BF)
    body = jnp.concatenate(
        [latent, turned_key, doc[:, None], jnp.zeros((rows, PACKW - 577), BF)], axis=1
    )
    foot = jnp.pad(doc[None, :], ((0, PACKR - rows - 1), (0, PACKW - rows)))
    pack = jnp.concatenate([body, foot], axis=0)
    down = ffn_down.T
    shard = jnp.concatenate([down[:, :DA], ffn_gate, ffn_value, down[:, DA:]], axis=1)
    gains = jnp.stack([norm1_gain, norm1_bias, norm2_gain, norm2_bias]).astype(F32)
    gains = jnp.pad(gains, ((0, 4), (0, 0)))
    taps = jnp.pad(jnp.concatenate([conv_gate, conv_value], axis=1).astype(F32), ((0, 5), (0, 0)))

    anyspec = pl.BlockSpec(memory_space=pl.ANY)
    vspec = pl.BlockSpec(memory_space=pltpu.VMEM)
    V = pltpu.VMEM
    return pl.pallas_call(
        layer_kernel,
        out_shape=jax.ShapeDtypeStruct((rows, CH), BF),
        in_specs=[anyspec] * 8 + [vspec] * 2,
        out_specs=vspec,
        scratch_shapes=[
            V((4, PACKR, PACKW), BF),
            V((ROWS, 1024), BF),
            V((ROWS, 1024), BF),
            V((512, 1024), BF),
            V((512, 1024), BF),
            V((1024, D), BF),
            V((ROWS, CH), BF),
            V((NZ, NX, 2, 32, LW), BF),
            V((NY, 8, CH), F32),
            V((ROWS, 1024), BF),
            V((8, ROWS, 128), F32),
            V((8, ROWS, 128), F32),
            V((8, ROWS, 128), F32),
            V((8 + ROWS, 128), F32),
            V((ROWS, CH), BF),
            V((ROWS, CH), BF),
            V((ROWS, CH), BF),
            V((HALF, CH), F32),
            V((HALF, CH), F32),
            V((ROWS, CH), F32),
            V((2, HALF, CH), BF),
            V((2, ROWS, CH), BF),
            V((2, HALF, CH), BF),
            V((2, ROWS, CH), BF),
            V((NY, ROWS, CH), BF),
            V((ROWS, D), BF),
            V((8 + ROWS, 2 * UNITS), F32),
            V((ROWS, UNITS), BF),
            V((1, 8, 2 * UNITS), F32),
            V((NY, 8, ROWS), F32),
            pltpu.SemaphoreType.DMA((8,)),
            pltpu.SemaphoreType.DMA((N_SEND,)),
            pltpu.SemaphoreType.DMA((N_RECV,)),
        ],
        compiler_params=pltpu.CompilerParams(
            collective_id=0, has_side_effects=True, vmem_limit_bytes=60 * 1024 * 1024
        ),
    )(pack, query_nope, turned_query, key_up, value_up, out_proj, residual, shard, gains, taps)


def solution(mesh):
    placed = (
        P("sp", "tp"),
        P("sp", "tp"),
        P("sp", "tp"),
        P("sp", None),
        P("sp", None),
        P("sp"),
        P(None, "tp"),
        P(None, "tp"),
        P("tp", None),
        P("tp"),
        P("tp"),
        P("sp", "tp"),
        P("sp", "tp"),
        P(None, "tp"),
        P(None, "tp"),
        P("tp", "sp"),
        P("tp"),
        P("tp"),
    )
    return jax.shard_map(
        local, mesh=mesh, in_specs=placed, out_specs=P("sp", "tp"), check_vma=False
    )
```

time: 250 us -> 150 us (0.60)
  Pallas kernels: 0 us -> 138 us
  matrix products: 67.5 us -> 0 us
  starting transfers between devices: 46.7 us -> 0 us
  waiting for transfers between devices: 46.2 us -> 0 us
  blocking collectives: 45.4 us -> 0 us
  other arithmetic: 22.2 us -> 3.96 us
  between operations: 14 us -> 0.26 us
    pallas_call x0 -> x1, Pallas kernels: none -> 138 us  [local(): pl.pallas_call(layer_kernel, out_shape=jax.ShapeDtypeStruct((rows, CH), B...]
    dot_general x9 -> x0, matrix products: 67.5 us -> none  [the longest x1 17.5 us: local(): jnp.einsum('hqk,khd->qhd', weights, values.reshape(window, head_count, VD...]
    all_to_all x2 -> x0, blocking collectives: 45.4 us -> none  [sum_at_owner(): lax.all_to_all(parts, axis, split_axis=0, concat_axis=0, tiled=True)]
    ppermute x12 -> x0, starting transfers between devices: 35.8 us -> none  [passed_along(): return lax.ppermute(value, axis, pairs)]
    all_to_all x3 -> x0, waiting for transfers between devices: 27 us -> none  [from_everyone(): return lax.all_to_all(copies, axis, split_axis=0, concat_axis=0, tiled=True)]
    ppermute x12 -> x0, waiting for transfers between devices: 18.5 us -> none  [passed_along(): return lax.ppermute(value, axis, pairs)]
    sub x1 -> x0, other arithmetic: 15.3 us -> none  [local(): weights = jnp.exp(scores - row_max)]
    all_to_all x3 -> x0, starting transfers between devices: 10.8 us -> none  [from_everyone(): return lax.all_to_all(copies, axis, split_axis=0, concat_axis=0, tiled=True)]
  transfers between devices with their start and end apart: 17 -> 0, of which waited for: 7 -> 0; matrix products, arithmetic and copies ran while one was open for 33% -> 0% of each run, Pallas kernels for 0% -> 0%
where the time goes in v1:
time: 150 us; the launch traced here: 147 us
  Pallas kernels  138 us (92%)
  local copies, waits for them, and re-layouts  4.95 us (3%)
  other arithmetic  3.96 us (3%)
    pallas_call x1, Pallas kernels, local(): pl.pallas_call(layer_kernel, out_shape=jax.ShapeDtypeStruct((rows, CH), B...  138 us
    unnamed x27, local copies, waits for them, and re-layouts  3.02 us

profile of v1, /device:TPU:6, one launch (start us, length us, event | category | flops | bytes accessed | tf_op | source)
XLA Modules:
  0.0 147.5 jit_solution(10952006421326779125)
XLA Ops:
  0.0 0.0 copy-start
  0.0 1.0 copy.26
  1.0 0.8 multiply_cosine_fusion
  1.9 0.1 copy.30
  2.0 0.1 copy.31
  2.1 0.0 copy-done
  2.1 0.2 copy.29
  2.3 0.1 convert.21
  2.4 0.1 subtract_convert_fusion
  2.5 0.0 copy-start.7
  2.5 0.0 copy-start.1
  2.5 0.1 fusion.3
  2.6 1.2 copy.33.qr_h
  3.8 0.0 copy-start.2
  3.8 0.0 copy-start.3
  3.8 0.0 copy-start.4
  3.8 0.0 copy-done.7
  3.8 0.1 broadcast_in_dim.16
  3.9 0.0 copy-start.5
  3.9 0.0 copy-start.6
  4.0 0.0 copy-done.1
  4.0 0.0 copy-start.8
  4.0 0.0 copy-start.9
  4.0 0.0 copy-start.10
  4.0 0.0 copy-start.11
  4.0 0.4 concatenate.19
  4.4 0.9 fusion.4.pack_h
  5.3 0.0 copy-done.2
  5.3 0.0 copy-done.3
  5.3 0.0 copy-done.4
  5.3 0.7 pad_maximum_fusion.wsh_h
  6.1 0.0 copy-done.5
  6.1 0.0 copy-done.6
  6.1 0.7 fusion.8.cv_ref
  6.7 0.0 copy-done.8
  6.7 0.0 copy-done.9
  6.7 0.0 copy-done.10
  6.8 0.0 copy-done.11
  6.8 0.6 fusion.16.gb_ref
  7.4 138.3 %shard_map.172 = bf16[384,512]{1,0:T(8,128)(2,1)} custom-call(bf16[400,640]{1,0:T(8,128)(2,1)} %fusion.4.pack_h, bf16[384,1024]{1,0:T(8,128)(2,1)} %qn_h.1, bf16[384,1024]{1,0:T(8,128)(2,1)} %copy.33.qr_h, bf16[512,1024]{1,0:T(8,128)(2,1)} %kup_h.1, bf16[512,1024]{1,0:T(8,128)(2,1)} %vup_h.1, bf16[1024,2048]{1,0:T(8,128)(2,1)} %op_h.1, ...), custom_call_target="tpu_custom_call" | custom-call | tf_op jit(solution)/shard_map/pallas_call | solution.py:558
  145.7 1.8 %copy.35 = bf16[384,512]{1,0:T(8,128)(2,1)} copy(bf16[384,512]{1,0:T(8,128)(2,1)} %shard_map.172) | data formatting | bytes 786432
  (12 shorter events, 0.1 us)
Async XLA Ops:
  0.0 2.1 %copy-start = (bf16[384,512]{1,0:T(8,128)(2,1)S(1)}, bf16[384,512]{1,0:T(8,128)(2,1)}, u32[]{:S(2)}) copy-start(bf16[384,512]{1,0:T(8,128)(2,1)} %param.20) | copy-start | bytes 1179652
  2.5 1.3 copy-start.7
  2.5 1.5 %copy-start.1 = (bf16[384,512]{1,0:T(8,128)(2,1)S(1)}, bf16[384,512]{1,0:T(8,128)(2,1)}, u32[]{:S(2)}) copy-start(bf16[384,512]{1,0:T(8,128)(2,1)} %param.21) | copy-start | bytes 1179652
  3.8 1.5 %copy-start.2 = (bf16[1408,32]{0,1:T(8,128)(2,1)S(1)}, bf16[1408,32]{0,1:T(8,128)(2,1)}, u32[]{:S(2)}) copy-start(bf16[1408,32]{0,1:T(8,128)(2,1)} %param.33) | copy-start | bytes 270340
  3.8 1.5 %copy-start.3 = (bf16[32,1408]{1,0:T(8,128)(2,1)S(1)}, bf16[32,1408]{1,0:T(8,128)(2,1)}, u32[]{:S(2)}) copy-start(bf16[32,1408]{1,0:T(8,128)(2,1)} %param.30) | copy-start | bytes 270340
  3.8 1.5 %copy-start.4 = (bf16[32,1408]{1,0:T(8,128)(2,1)S(1)}, bf16[32,1408]{1,0:T(8,128)(2,1)}, u32[]{:S(2)}) copy-start(bf16[32,1408]{1,0:T(8,128)(2,1)} %param.29) | copy-start | bytes 270340
  3.9 2.1 %copy-start.5 = (bf16[3,1408]{1,0:T(4,128)(2,1)S(1)}, bf16[3,1408]{1,0:T(4,128)(2,1)}, u32[]{:S(2)}) copy-start(bf16[3,1408]{1,0:T(4,128)(2,1)} %param.32) | copy-start | bytes 25348
  3.9 2.1 %copy-start.6 = (bf16[3,1408]{1,0:T(4,128)(2,1)S(1)}, bf16[3,1408]{1,0:T(4,128)(2,1)}, u32[]{:S(2)}) copy-start(bf16[3,1408]{1,0:T(4,128)(2,1)} %param.31) | copy-start | bytes 25348
  4.0 2.7 %copy-start.8 = (bf16[512]{0:T(512)(128)(2,1)S(1)}, bf16[512]{0:T(512)(128)(2,1)}, u32[]{:S(2)}) copy-start(bf16[512]{0:T(512)(128)(2,1)} %param.27) | copy-start | bytes 3076
  4.0 2.7 %copy-start.9 = (bf16[512]{0:T(512)(128)(2,1)S(1)}, bf16[512]{0:T(512)(128)(2,1)}, u32[]{:S(2)}) copy-start(bf16[512]{0:T(512)(128)(2,1)} %param.28) | copy-start | bytes 3076
  4.0 2.7 %copy-start.10 = (bf16[512]{0:T(512)(128)(2,1)S(1)}, bf16[512]{0:T(512)(128)(2,1)}, u32[]{:S(2)}) copy-start(bf16[512]{0:T(512)(128)(2,1)} %param.34) | copy-start | bytes 3076
  4.0 2.7 %copy-start.11 = (bf16[512]{0:T(512)(128)(2,1)S(1)}, bf16[512]{0:T(512)(128)(2,1)}, u32[]{:S(2)}) copy-start(bf16[512]{0:T(512)(128)(2,1)} %param.35) | copy-start | bytes 3076

commit v2 on v1

--- a/solution.py
+++ b/solution.py
@@ -27,7 +27,10 @@
 LA = DA + UNITS
 LW = 3 * UNITS
 PACKW = 640
-PACKR = 400
+GROUP = 4
+N_SEND = 96
+N_RECV = 96
+S_ALT = N_SEND - 4
 MESH = pl.DeviceIdType.MESH
 BF = jnp.bfloat16
 F32 = jnp.float32
@@ -42,9 +45,10 @@
 
 
 def layer_kernel(
-    pack_h, qn_h, qr_h, kup_h, vup_h, op_h, res_h, wsh_h, gb_ref, cv_ref,
+    lat_h, qn_h, qr_h, kup_h, vup_h, op_h, res_h, gate_h, value_h, down_h,
+    key_ref, cos_ref, sin_ref, gb_ref, cg_ref, cv_ref,
     out_ref,
-    packs, qn, qr, kup, vup, op, res, w, gbs, att, acc, mrun, lrun, dcol,
+    packs, qn, qraw, qr, kup, vup, op, res, w, gbs, att, acc, mrun, lrun, dcol, docs, bias,
     sa, sp_buf, sm_buf, pfp, pfm, own, ra, rb, ra2, rb2, m4, nf, gv, hid, stat, stats,
     lsem, ssem, rsem,
 ):
@@ -77,22 +81,45 @@
         d.start()
         local.append(d)
         return d
-    f_pack = fetch(pack_h, packs.at[0])
-    f_w = fetch(wsh_h, w.at[z, x, c])
+    f_lat = fetch(lat_h, packs.at[0, :, pl.ds(0, 512)])
+    mine = w.at[z, x, c]
+    f_w = [
+        fetch(gate_h, mine.at[:, pl.ds(DA, UNITS)]),
+        fetch(value_h, mine.at[:, pl.ds(LA, UNITS)]),
+        fetch(down_h.at[:, pl.ds(0, DA)], mine.at[:, pl.ds(0, DA)]),
+        fetch(down_h.at[:, pl.ds(DA, UNITS - DA)], mine.at[:, pl.ds(LA + UNITS, UNITS - DA)]),
+    ]
+    f_qr = fetch(qr_h, qraw)
     f_kup = fetch(kup_h, kup)
     f_qn = fetch(qn_h, qn)
-    f_qr = fetch(qr_h, qr)
     f_vup = fetch(vup_h, vup)
     f_op = fetch(op_h, op)
     f_res = fetch(res_h, res)
 
+    lane = lax.broadcasted_iota(jnp.int32, (ROWS, 128), 1)
+    front = lax.rem(lane, ROPE) < ROPE // 2
+
+    def turned(v):
+        swapped = jnp.where(front, pltpu.roll(v, 128 - ROPE // 2, 1), pltpu.roll(v, ROPE // 2, 1))
+        return v * cos_ref[...] + swapped * sin_ref[...]
+
+    key = key_ref[...].astype(F32)
+    packs[0, :, 512:640] = turned(jnp.concatenate([key, key], axis=0).T).astype(BF)
+    docs[0] = jnp.broadcast_to(gb_ref[4:5, 0:ROWS], (8, ROWS))
+    def doc_column(slot):
+        return jnp.concatenate([docs[slot], jnp.zeros((120, ROWS), F32)], axis=0).T[:, 0:1]
+
     barrier = pltpu.get_barrier_semaphore()
-    peers = (xp, xm, zp, zm, sib, yp, ym, yy, nextc, prevc, nexto, prevo)
+    peers = (
+        xp, xm, zp, zm, sib, yp, ym, yy, nextc, prevc, nexto, prevo,
+        chip(k + 2, 1 - c), chip(k - 2, 1 - c),
+    )
     for p in peers:
         pl.semaphore_signal(barrier, inc=1, device_id=p, device_id_type=MESH)
     pl.semaphore_wait(barrier, len(peers))
 
     sends = []
+    zero_only = []
     names = {}
 
     def rid(name):
@@ -105,6 +132,12 @@
         )
         sends.append(d)
         return d
+
+    def copy_at(src, dst, to, name, at):
+        return pltpu.make_async_remote_copy(
+            src_ref=src, dst_ref=dst, send_sem=ssem.at[at],
+            recv_sem=rsem.at[rid(name)], device_id=to, device_id_type=MESH,
+        )
 
     def send(src, dst, to, name):
         copy_to(src, dst, to, name).start()
@@ -213,124 +246,173 @@
         arrive(xb(1, 1 - c), "sx1p")
         arrive(xb(2, 1 - c), "sx2")
 
-    f_w.wait()
+    QR = ROWS // NY
+
+    def quarter(slot, dy, lo=0, n=QR):
+        return packs.at[slot, pl.ds(pl.multiple_of(wrap(y + dy, NY) * QR + lo, 16), n)]
+
+    def spread(slot, tag):
+        def one():
+            arrive(quarter(slot, 0), tag)
+            same(quarter(slot, 0), yp, tag + "1m")
+            same(quarter(slot, 0), ym, tag + "1p")
+
+        def two():
+            arrive(quarter(slot, -1), tag + "1m")
+            same(quarter(slot, -1, 0, QR // 2), yp, tag + "2m")
+            arrive(quarter(slot, 1), tag + "1p")
+            same(quarter(slot, 1, QR // 2, QR // 2), ym, tag + "2p")
+
+        def three():
+            arrive(quarter(slot, 2, 0, QR // 2), tag + "2m")
+            arrive(quarter(slot, 2, QR // 2, QR // 2), tag + "2p")
+
+        return one, two, three
+
+    f_lat.wait()
+    send(quarter(0, 0), quarter(2, 0), nextc, "l2")
+    send(docs.at[0], docs.at[2], nextc, "d2")
+    for d in f_w:
+        d.wait()
     a_start()
     b_start()
-    f_pack.wait()
-    third_at = len(sends)
-    third = copy_to(packs.at[0], packs.at[1], sib, "l1")
 
     @pl.when(c == 0)
     def _():
-        third.start()
-
-    send(packs.at[0], packs.at[2], nextc, "l2")
+        copy_at(packs.at[0], packs.at[1], sib, "l1", S_ALT).start()
+        copy_at(docs.at[0], docs.at[1], sib, "d1", S_ALT + 1).start()
+        copy_at(docs.at[0], docs.at[3], nexto, "d3", S_ALT + 2).start()
+
+    @pl.when(c == 1)
+    def _():
+        copy_at(docs.at[0], docs.at[1], nexto, "d1", S_ALT + 1).start()
+        copy_at(docs.at[0], docs.at[3], chip(k + 2, 0), "d3", S_ALT + 2).start()
+
     send(gb_ref, gbs.at[y], yp, "gm")
     send(gb_ref, gbs.at[y], ym, "gp")
     send(gb_ref, gbs.at[y], yy, "g2")
-
-    def doc_column(slot):
-        return packs[slot, 0:ROWS, 512:640].astype(F32)[:, ROPE : ROPE + 1]
-
     dcol[8 : 8 + ROWS, :] = jnp.broadcast_to(doc_column(0), (ROWS, 128))
+    f_qr.wait()
+    for t in range(4):
+        v = turned(qraw[:, t * 128 : t * 128 + 128].astype(F32))
+        qr[:, t * 256 : t * 256 + 128] = jnp.where(lane < ROPE, v, 0.0).astype(BF)
+        qr[:, t * 256 + 128 : t * 256 + 256] = jnp.where(lane >= ROPE, v, 0.0).astype(BF)
 
     def attend(slot, back, kind, first=False, last=False):
-        exists = sp >= back
-
-        def body(pair, carry):
-            off = pl.multiple_of(pair * 256, 256)
-            lat = packs[slot, 0:ROWS, 0:512]
-            kr = packs[slot, 0:ROWS, 512:640]
-            kdoc = packs[slot, ROWS:PACKR, 0:ROWS].astype(F32)[0:1, :]
-            kdoc = jnp.where(exists, kdoc, -1.0)
-            k2 = dot(lat, kup[:, pl.ds(off, 256)]).astype(BF)
-            v2 = dot(lat, vup[:, pl.ds(off, 256)]).astype(BF)
-            for hh in range(2):
-                h = pair * 2 + hh
-                lanes = pl.ds(pl.multiple_of(off + hh * 128, 128), 128)
-                kk = jnp.concatenate([k2[:, hh * 128 : hh * 128 + 128], kr], axis=1)
-                vv = v2[:, hh * 128 : hh * 128 + 128]
-                for qi in range(3):
-                    r0 = qi * 128
-                    rows = pl.ds(r0, 128)
-                    lo, hi = 0, ROWS
-                    if kind == "diag":
-                        hi = r0 + 128
-                    if kind == "far":
-                        lo = r0
-                    q = jnp.concatenate([qn[rows, lanes], qr[rows, lanes]], axis=1)
-                    s = dot_nt(q, kk[lo:hi])
-                    qdoc = dcol[8 + r0 : 8 + r0 + 128, 0:1]
-                    ok = qdoc == kdoc[:, lo:hi]
-                    if kind == "diag":
-                        qi_pos = lax.broadcasted_iota(jnp.int32, s.shape, 0) + r0
-                        ki_pos = lax.broadcasted_iota(jnp.int32, s.shape, 1)
-                        ok = ok & (ki_pos <= qi_pos)
-                    s = jnp.where(ok, s, masked_score)
-                    mx = jnp.max(s, axis=1, keepdims=True)
-                    if first:
-                        p = jnp.exp2((s - mx) * SCALE2)
-                        total = jnp.broadcast_to(jnp.sum(p, axis=1, keepdims=True), (128, 128))
-                        o = dot(p.astype(BF), vv[lo:hi])
-                        mnew = jnp.broadcast_to(mx, (128, 128))
-                    else:
-                        mold = mrun[h, rows, :]
-                        mnew = jnp.maximum(mold, mx)
-                        alpha = jnp.exp2((mold - mnew) * SCALE2)
-                        p = jnp.exp2((s - mnew[:, 0:1]) * SCALE2)
-                        total = lrun[h, rows, :] * alpha + jnp.sum(p, axis=1, keepdims=True)
-                        o = acc[h, rows, :] * alpha + dot(p.astype(BF), vv[lo:hi])
-                    if last:
-                        att[rows, lanes] = (o / total).astype(BF)
-                    else:
-                        mrun[h, rows, :] = mnew
-                        lrun[h, rows, :] = total
-                        acc[h, rows, :] = o
+        kdoc = jnp.where(sp >= back, docs[slot, 0:1, :], -1.0)
+        ok = dcol[8 : 8 + ROWS, 0:1] == kdoc
+        if kind == "diag":
+            qi_pos = lax.broadcasted_iota(jnp.int32, (ROWS, ROWS), 0)
+            ki_pos = lax.broadcasted_iota(jnp.int32, (ROWS, ROWS), 1)
+            ok = ok & (ki_pos <= qi_pos)
+        bias[...] = jnp.where(ok, 0.0, masked_score)
+        ones = jnp.ones((ROWS, 128), BF)
+
+        def body(group, carry):
+            lat = packs[slot, :, 0:512]
+            kr = packs[slot, :, 512:640]
+            lanes, states, results = [], [], []
+            for hh in range(GROUP):
+                h = group * GROUP + hh
+                lanes.append(pl.ds(pl.multiple_of(h * 128, 128), 128))
+                if not first:
+                    states.append((mrun[h], lrun[h], acc[h]))
+            for hh in range(GROUP):
+                if hh % 2 == 0:
+                    both = pl.ds(pl.multiple_of((group * GROUP + hh) * 128, 256), 256)
+                    k2 = dot(lat, kup[:, both]).astype(BF)
+                    v2 = dot(lat, vup[:, both]).astype(BF)
+                part = slice(hh % 2 * 128, hh % 2 * 128 + 128)
+                kk = jnp.concatenate([k2[:, part], kr], axis=1)
+                vv = jnp.concatenate([v2[:, part], ones], axis=1)
+                q = jnp.concatenate([qn[:, lanes[hh]], qr[:, lanes[hh]]], axis=1)
+                s = dot_nt(q, kk) + bias[...]
+                mx = jnp.max(s, axis=1, keepdims=True)
+                if first:
+                    mnew = jnp.broadcast_to(mx, (ROWS, 128))
+                else:
+                    mnew = jnp.maximum(states[hh][0], mx)
+                p = jnp.exp2((s - mnew[:, 0:1]) * SCALE2)
+                o = dot(p.astype(BF), vv)
+                o, total = o[:, 0:128], o[:, 128:256]
+                if not first:
+                    alpha = jnp.exp2((states[hh][0] - mnew) * SCALE2)
+                    total = states[hh][1] * alpha + total
+                    o = states[hh][2] * alpha + o
+                results.append((mnew, total, o))
+            for hh in range(GROUP):
+                h = group * GROUP + hh
+                mnew, total, o = results[hh]
+                if last:
+                    att[:, lanes[hh]] = (o / total).astype(BF)
+                else:
+                    mrun[h] = mnew
+                    lrun[h] = total
+                    acc[h] = o
             return carry
 
-        lax.fori_loop(0, 4, body, 0)
+        lax.fori_loop(0, 8 // GROUP, body, 0)
 
     f_kup.wait()
     f_qn.wait()
-    f_qr.wait()
     f_vup.wait()
+    slot_two = spread(2, "l2")
+    slot_three = spread(3, "l3")
     attend(0, 0, "diag", first=True)
+    slot_two[0]()
+
+    @pl.when(c == 1)
+    def _():
+        copy_at(quarter(2, 0), quarter(3, 0), nexto, "l3", S_ALT).start()
+
     a_one()
     b_step(1)
+    slot_two[1]()
+    b_step(2)
+    slot_two[2]()
+
+    @pl.when(c == 0)
+    def _():
+        copy_at(packs.at[2], packs.at[3], sib, "s3", S_ALT + 3).start()
+        before = len(sends)
+        slot_three[0]()
+        for i in range(before, len(sends)):
+            zero_only.append(i)
+            sends[i] = None
+
+    @pl.when(c == 1)
+    def _():
+        copy_at(packs.at[2], packs.at[1], sib, "l1", S_ALT + 3).start()
+
+    b_step(3)
+    arrive(docs.at[2], "d2")
+    attend(2, 2, "full")
     a_two()
-    b_step(2)
-    b_step(3)
-    arrive(packs.at[2], "l2")
-    hand = copy_to(packs.at[2], packs.at[3 - 2 * c], sib, "l1")
-    hand_three = pltpu.make_async_remote_copy(
-        src_ref=packs.at[2], dst_ref=packs.at[3], send_sem=ssem.at[len(sends) - 1],
-        recv_sem=rsem.at[rid("l3")], device_id=sib, device_id_type=MESH,
-    )
-    relay = pltpu.make_async_remote_copy(
-        src_ref=packs.at[2], dst_ref=packs.at[3], send_sem=ssem.at[third_at],
-        recv_sem=rsem.at[rid("l3")], device_id=nexto, device_id_type=MESH,
-    )
-    hand_one = pltpu.make_async_remote_copy(
-        src_ref=packs.at[2], dst_ref=packs.at[1], send_sem=ssem.at[len(sends) - 1],
-        recv_sem=rsem.at[rid("l1")], device_id=sib, device_id_type=MESH,
-    )
-
-    @pl.when(c == 0)
-    def _():
-        hand_three.start()
-
-    @pl.when(c == 1)
-    def _():
-        hand_one.start()
-        relay.start()
-
-    attend(2, 2, "full")
     b_turn()
     arrive(packs.at[1], "l1")
+    arrive(docs.at[1], "d1")
     before = jnp.where(sp >= 1, doc_column(1)[ROWS - 8 : ROWS, :], -1.0)
     dcol[0:8, :] = jnp.broadcast_to(before, (8, 128))
+
+    @pl.when(c == 0)
+    def _():
+        before = len(sends)
+        slot_three[1]()
+        for i in range(before, len(sends)):
+            zero_only.append(i)
+            sends[i] = None
+
     attend(1, 1, "full")
-    arrive(packs.at[3], "l3")
+    arrive(docs.at[3], "d3")
+
+    @pl.when(c == 0)
+    def _():
+        slot_three[2]()
+
+    @pl.when(c == 1)
+    def _():
+        arrive(packs.at[3], "s3")
+
     attend(3, 3, "far", last=True)
     a_step(1)
 
@@ -445,19 +527,16 @@
         two = (dcol[6 + r0 : 6 + r0 + 128, :] == here).astype(F32)
 
         def cols(j, carry):
-            def mix(base):
+            def mix(taps, base):
                 lanes = pl.ds(pl.multiple_of(base + j * 128, 128), 128)
                 a0 = gv[6 + r0 : 6 + r0 + 128, lanes]
                 a1 = gv[7 + r0 : 7 + r0 + 128, lanes]
                 a2 = gv[8 + r0 : 8 + r0 + 128, lanes]
-                return (
-                    cv_ref[0:1, lanes] * a0 * two
-                    + cv_ref[1:2, lanes] * a1 * one
-                    + cv_ref[2:3, lanes] * a2
-                )
-
-            g = mix(0)
-            v = mix(UNITS)
+                t = taps[:, pl.ds(pl.multiple_of(j * 128, 128), 128)].astype(F32)
+                return t[0:1] * a0 * two + t[1:2] * a1 * one + t[2:3] * a2
+
+            g = mix(cg_ref, 0)
+            v = mix(cv_ref, UNITS)
             act = 0.5 * g * (1.0 + jnp.tanh(0.7978845608028654 * (g + 0.044715 * (g * g * g))))
             hid[r0 : r0 + 128, pl.ds(pl.multiple_of(j * 128, 128), 128)] = (v * act).astype(BF)
             return carry
@@ -482,7 +561,6 @@
         residual_scale * nf[:, pl.ds(pl.multiple_of(y * CH, CH), CH)].astype(F32) + total_two
     )
     own[...] = mixed
-    lane = lax.broadcasted_iota(jnp.int32, (ROWS, 128), 1)
     s = jnp.sum(mixed, axis=1, keepdims=True)
     q = jnp.sum(mixed * mixed, axis=1, keepdims=True)
     both = jnp.where(lane == 0, s, jnp.where(lane == 1, q, 0.0))
@@ -498,32 +576,30 @@
     s = back[:, 0:1] / D
     q = back[:, 1:2] / D
     r = lax.rsqrt(q - s * s + norm_eps)
-    out_ref[...] = ((own[...] - s) * r * gb_ref[2:3, :] + gb_ref[3:4, :]).astype(BF)
-    settle(sends[:mark])
+    out_ref[...] = ((own[...] - s) * r * gbs[y, 2:3, :] + gbs[y, 3:4, :]).astype(BF)
+    settle(d for d in sends[:mark] if d is not None)
     settle(sends[mark + 6 :])
-
-
-N_SEND = 72
-N_RECV = 72
+    copy_at(docs.at[0], docs.at[1], sib, "d1", S_ALT + 1).wait_send()
+    copy_at(docs.at[0], docs.at[3], sib, "d3", S_ALT + 2).wait_send()
+    copy_at(packs.at[2], packs.at[3], sib, "s3", S_ALT + 3).wait_send()
+
+    @pl.when(c == 0)
+    def _():
+        copy_at(packs.at[0], packs.at[1], sib, "l1", S_ALT).wait_send()
+        for i, at in enumerate(zero_only):
+            part = quarter(3, 0, 0, QR if i < 2 else QR // 2)
+            copy_at(part, part, yp, "l3", at).wait_send()
+
+    @pl.when(c == 1)
+    def _():
+        copy_at(quarter(2, 0), quarter(3, 0), nexto, "l3", S_ALT).wait_send()
 
 
 def tables(positions):
     frequencies = 1.0 / rope_base_freq ** (jnp.arange(0, ROPE, 2, dtype=jnp.float32) / ROPE)
-    angles = positions.astype(jnp.float32)[:, None] * frequencies[None, :]
-    return (jnp.cos(angles), jnp.sin(angles))
-
-
-def rotate(vectors, cosine, sine_table):
-    half_width = vectors.shape[-1] // 2
-    front_half = vectors[..., :half_width]
-    back_half = vectors[..., half_width:]
-    return jnp.concatenate(
-        [
-            front_half * cosine - back_half * sine_table,
-            front_half * sine_table + back_half * cosine,
-        ],
-        axis=-1,
-    )
+    angles = positions.astype(jnp.float32)[:, None] * jnp.tile(frequencies, 4)[None, :]
+    sign = jnp.where(jnp.arange(128) % ROPE < ROPE // 2, -1.0, 1.0).astype(jnp.float32)
+    return (jnp.cos(angles), jnp.sin(angles) * sign[None, :])
 
 
 def local(
@@ -532,25 +608,12 @@
     norm2_gain, norm2_bias,
 ):
     rows = latent.shape[0]
-    heads = query_nope.shape[1] // NOPE
     positions = lax.axis_index("sp") * rows + jnp.arange(rows, dtype=jnp.int32)
     cosine, sine = tables(positions)
-    turned_key = rotate(rope_key.astype(F32), cosine, sine).astype(BF)
-    turned_query = rotate(
-        query_rope.astype(F32).reshape(rows, heads, ROPE), cosine[:, None], sine[:, None]
-    ).astype(BF)
-    turned_query = jnp.pad(turned_query, ((0, 0), (0, 0), (0, 128 - ROPE))).reshape(rows, heads * 128)
-    doc = doc_ids.astype(BF)
-    body = jnp.concatenate(
-        [latent, turned_key, doc[:, None], jnp.zeros((rows, PACKW - 577), BF)], axis=1
-    )
-    foot = jnp.pad(doc[None, :], ((0, PACKR - rows - 1), (0, PACKW - rows)))
-    pack = jnp.concatenate([body, foot], axis=0)
-    down = ffn_down.T
-    shard = jnp.concatenate([down[:, :DA], ffn_gate, ffn_value, down[:, DA:]], axis=1)
-    gains = jnp.stack([norm1_gain, norm1_bias, norm2_gain, norm2_bias]).astype(F32)
-    gains = jnp.pad(gains, ((0, 4), (0, 0)))
-    taps = jnp.pad(jnp.concatenate([conv_gate, conv_value], axis=1).astype(F32), ((0, 5), (0, 0)))
+    doc = jnp.pad(doc_ids.astype(BF), (0, CH - rows))
+    none = jnp.zeros((3 * CH,), BF)
+    vectors = jnp.concatenate([norm1_gain, norm1_bias, norm2_gain, norm2_bias, doc, none])
+    vectors = vectors.astype(F32).reshape(8, CH)
 
     anyspec = pl.BlockSpec(memory_space=pl.ANY)
     vspec = pl.BlockSpec(memory_space=pltpu.VMEM)
@@ -558,11 +621,12 @@
     return pl.pallas_call(
         layer_kernel,
         out_shape=jax.ShapeDtypeStruct((rows, CH), BF),
-        in_specs=[anyspec] * 8 + [vspec] * 2,
+        in_specs=[anyspec] * 10 + [vspec] * 6,
         out_specs=vspec,
         scratch_shapes=[
-            V((4, PACKR, PACKW), BF),
+            V((4, ROWS, PACKW), BF),
             V((ROWS, 1024), BF),
+            V((ROWS, CH), BF),
             V((ROWS, 1024), BF),
             V((512, 1024), BF),
             V((512, 1024), BF),
@@ -575,6 +639,8 @@
             V((8, ROWS, 128), F32),
             V((8, ROWS, 128), F32),
             V((8 + ROWS, 128), F32),
+            V((4, 8, ROWS), F32),
+            V((ROWS, ROWS), F32),
             V((ROWS, CH), BF),
             V((ROWS, CH), BF),
             V((ROWS, CH), BF),
@@ -591,14 +657,18 @@
             V((ROWS, UNITS), BF),
             V((1, 8, 2 * UNITS), F32),
             V((NY, 8, ROWS), F32),
-            pltpu.SemaphoreType.DMA((8,)),
+            pltpu.SemaphoreType.DMA((11,)),
             pltpu.SemaphoreType.DMA((N_SEND,)),
             pltpu.SemaphoreType.DMA((N_RECV,)),
         ],
         compiler_params=pltpu.CompilerParams(
             collective_id=0, has_side_effects=True, vmem_limit_bytes=60 * 1024 * 1024
         ),
-    )(pack, query_nope, turned_query, key_up, value_up, out_proj, residual, shard, gains, taps)
+    )(
+        latent, query_nope, query_rope, key_up, value_up, out_proj, residual,
+        ffn_gate, ffn_value, ffn_down.T, rope_key.T, cosine, sine,
+        vectors, conv_gate, conv_value,
+    )
 
 
 def solution(mesh):

time: 150 us -> 119 us (0.79)
  the two profiles are of different devices: /device:TPU:6 before, /device:TPU:64 now
where the time goes in v2:
time: 119 us
  Pallas kernels  110 us (92%)
  local copies, waits for them, and re-layouts  6.37 us (5%)
  other arithmetic  2.22 us (2%)
    pallas_call x1, Pallas kernels, local(): pl.pallas_call(layer_kernel, out_shape=jax.ShapeDtypeStruct((rows, CH), B...  110 us
    unnamed x6, local copies, waits for them, and re-layouts  5.41 us

profile of v2, /device:TPU:64, one launch (start us, length us, event | category | flops | bytes accessed | tf_op | source)
XLA Modules:
  0.0 118.9 jit_solution(9909060212641453767)
XLA Ops:
  0.0 0.7 convert_element_type.20
  0.7 0.1 mul.31
  0.8 0.9 dynamic-update-slice
  1.7 0.9 dynamic-update-slice.1
  2.5 0.9 dynamic-update-slice.2
  3.4 0.9 dynamic-update-slice.3
  4.3 0.2 dynamic-update-slice.4
  4.5 0.2 dynamic-update-slice.5
  4.7 0.6 reshape.27.gb_ref
  5.3 1.5 %fusion = (f32[384,128]{1,0:T(8,128)}, f32[384,128]{1,0:T(8,128)}) fusion(f32[128]{0:T(128)S(1)} %compare_select_fusion, f32[128]{0:T(128)S(1)} %mul.31, f32[384]{0:T(512)S(1)} %add_convert_fusion), kind=kLoop, calls=%fused_computation.2 | loop fusion | flops 98304 | bytes 395776 | tf_op jit(solution)/shard_map/mul | solution.py:602
  6.8 110.3 %shard_map.172 = bf16[384,512]{1,0:T(8,128)(2,1)} custom-call(bf16[384,512]{1,0:T(8,128)(2,1)} %lat_h.1, bf16[384,1024]{1,0:T(8,128)(2,1)} %qn_h.1, bf16[384,512]{1,0:T(8,128)(2,1)} %qr_h.1, bf16[512,1024]{1,0:T(8,128)(2,1)} %kup_h.1, bf16[512,1024]{1,0:T(8,128)(2,1)} %vup_h.1, bf16[1024,2048]{1,0:T(8,128)(2,1)} %op_h.1, bf16[384,512]{1,0:T(8,128)(2,1)} %res_h.1, ...), custom_call_target="tpu_custom_call" | custom-call | tf_op jit(solution)/shard_map/pallas_call | solution.py:621
  117.2 1.8 %copy.26 = bf16[384,512]{1,0:T(8,128)(2,1)} copy(bf16[384,512]{1,0:T(8,128)(2,1)} %shard_map.172) | data formatting | bytes 786432
  (7 shorter events, 0.0 us)

commit v3 on v2

--- a/solution.py
+++ b/solution.py
@@ -1,5 +1,6 @@
 import jax
 import jax.numpy as jnp
+import numpy as np
 from jax import lax
 from jax.experimental import pallas as pl
 from jax.experimental.pallas import tpu as pltpu
@@ -23,13 +24,13 @@
 HALF = ROWS // 2
 CH = 512
 UNITS = 1408
-DA = 512
+DA = 256
 LA = DA + UNITS
 LW = 3 * UNITS
 PACKW = 640
 GROUP = 4
-N_SEND = 96
-N_RECV = 96
+N_SEND = 128
+N_RECV = 128
 S_ALT = N_SEND - 4
 MESH = pl.DeviceIdType.MESH
 BF = jnp.bfloat16
@@ -46,8 +47,9 @@
 
 def layer_kernel(
     lat_h, qn_h, qr_h, kup_h, vup_h, op_h, res_h, gate_h, value_h, down_h,
-    key_ref, cos_ref, sin_ref, gb_ref, cg_ref, cv_ref,
+    key_h, g1_h, b1_h, g2_h, b2_h, doc_h, cg_h, cv_h, freq_h,
     out_ref,
+    key_ref, v0, v1, v2, v3, doc_ref, cg_ref, cv_ref, freq_ref, gb_ref, cos_ref, sin_ref,
     packs, qn, qraw, qr, kup, vup, op, res, w, gbs, att, acc, mrun, lrun, dcol, docs, bias,
     sa, sp_buf, sm_buf, pfp, pfm, own, ra, rb, ra2, rb2, m4, nf, gv, hid, stat, stats,
     lsem, ssem, rsem,
@@ -81,6 +83,15 @@
         d.start()
         local.append(d)
         return d
+    f_small = [
+        fetch(key_h, key_ref),
+        fetch(freq_h, freq_ref),
+        fetch(doc_h, doc_ref),
+        fetch(g1_h, v0),
+        fetch(b1_h, v1),
+        fetch(g2_h, v2),
+        fetch(b2_h, v3),
+    ]
     f_lat = fetch(lat_h, packs.at[0, :, pl.ds(0, 512)])
     mine = w.at[z, x, c]
     f_w = [
@@ -93,21 +104,9 @@
     f_kup = fetch(kup_h, kup)
     f_qn = fetch(qn_h, qn)
     f_vup = fetch(vup_h, vup)
+    f_taps = [fetch(cg_h, cg_ref), fetch(cv_h, cv_ref)]
     f_op = fetch(op_h, op)
     f_res = fetch(res_h, res)
-
-    lane = lax.broadcasted_iota(jnp.int32, (ROWS, 128), 1)
-    front = lax.rem(lane, ROPE) < ROPE // 2
-
-    def turned(v):
-        swapped = jnp.where(front, pltpu.roll(v, 128 - ROPE // 2, 1), pltpu.roll(v, ROPE // 2, 1))
-        return v * cos_ref[...] + swapped * sin_ref[...]
-
-    key = key_ref[...].astype(F32)
-    packs[0, :, 512:640] = turned(jnp.concatenate([key, key], axis=0).T).astype(BF)
-    docs[0] = jnp.broadcast_to(gb_ref[4:5, 0:ROWS], (8, ROWS))
-    def doc_column(slot):
-        return jnp.concatenate([docs[slot], jnp.zeros((120, ROWS), F32)], axis=0).T[:, 0:1]
 
     barrier = pltpu.get_barrier_semaphore()
     peers = (
@@ -116,6 +115,28 @@
     )
     for p in peers:
         pl.semaphore_signal(barrier, inc=1, device_id=p, device_id_type=MESH)
+    lane = lax.broadcasted_iota(jnp.int32, (ROWS, 128), 1)
+    front = lax.rem(lane, ROPE) < ROPE // 2
+
+    def turned(v):
+        swapped = jnp.where(front, pltpu.roll(v, 128 - ROPE // 2, 1), pltpu.roll(v, ROPE // 2, 1))
+        return v * cos_ref[...] + swapped * sin_ref[...]
+
+    for d in f_small:
+        d.wait()
+    place = lax.broadcasted_iota(jnp.int32, (ROWS, 128), 0) + sp * ROWS
+    angle = place.astype(F32) * freq_ref[0:1, :]
+    cos_ref[...] = jnp.cos(angle)
+    sin_ref[...] = jnp.where(front, -1.0, 1.0) * jnp.sin(angle)
+    key = key_ref[...].astype(F32)
+    packs[0, :, 512:640] = turned(jnp.concatenate([key, key], axis=0).T).astype(BF)
+    docs[0] = jnp.broadcast_to(doc_ref[...].astype(F32).reshape(1, ROWS), (8, ROWS))
+    gb_ref[...] = jnp.concatenate(
+        [v[...].astype(F32).reshape(1, CH) for v in (v0, v1, v2, v3)] + [jnp.zeros((4, CH), F32)], axis=0
+    )
+    def doc_column(slot):
+        return jnp.concatenate([docs[slot], jnp.zeros((120, ROWS), F32)], axis=0).T[:, 0:1]
+
     pl.semaphore_wait(barrier, len(peers))
 
     sends = []
@@ -161,8 +182,10 @@
         return w.at[pl.ds(lo, n), wrap(x + dx, NX), cc, :, pl.ds(LA, LW - LA)]
 
     BH = (LW - LA) // 2
-    HZ = NZ // 2
     HX = NX // 2
+
+    def bp(dz, dx):
+        return w.at[wrap(z + dz, NZ), wrap(x + dx, NX), c, :, pl.ds(LA, LW - LA)]
 
     def same(ref, to, name):
         send(ref, ref, to, name)
@@ -171,20 +194,30 @@
         same(wa(0, 0), xp, "a1m")
         same(wa(0, 0), xm, "a1p")
 
+    def za_piece(dx):
+        same(wa(0, dx), zp, f"z1m{dx}")
+        same(wa(0, dx), zm, f"z1p{dx}")
+
     def a_one():
         arrive(wa(0, 1), "a1p")
         same(wa(0, 1), xm, "a2p")
+        za_piece(1)
 
     def a_two():
         arrive(wa(0, -1), "a1m")
+        za_piece(-1)
         arrive(wa(0, 2), "a2p")
-        same(za(0, c), zp, "z1m")
-        same(za(0, c), zm, "z1p")
+        za_piece(2)
         same(za(0, c), sib, "sz0")
 
     def a_step(s):
-        arrive(za(-s, c), f"z{s}m")
-        arrive(za(s, c), f"z{s}p")
+        if s == 1:
+            for dx in (0, 1, -1, 2):
+                arrive(wa(-1, dx), f"z1m{dx}")
+                arrive(wa(1, dx), f"z1p{dx}")
+        else:
+            arrive(za(-s, c), f"z{s}m")
+            arrive(za(s, c), f"z{s}p")
         if s < 3:
             same(za(-s, c), zp, f"z{s + 1}m")
             same(za(s, c), zm, f"z{s + 1}p")
@@ -205,6 +238,10 @@
             arrive(za(-s, 1 - c), f"sz{s}m")
             arrive(za(s, 1 - c), f"sz{s}p")
         arrive(za(4, 1 - c), "sz4")
+
+    def bx_piece(dz):
+        same(bp(dz, 0), xp, f"x1m{dz}")
+        same(bp(dz, 0), xm, f"x1p{dz}")
 
     def b_start():
         same(wb(0), zp, "b1m")
@@ -219,26 +256,39 @@
         else:
             same(wb(-s, LA, BH), zp, "b4m")
             same(wb(s, LA + BH, BH), zm, "b4p")
+        bx_piece(-s)
+        bx_piece(s)
 
     def b_turn():
         arrive(wb(4, LA, BH), "b4m")
         arrive(wb(4, LA + BH, BH), "b4p")
-        same(xb(0, c), xp, "x1m")
-        same(xb(0, c), xm, "x1p")
+        bx_piece(4)
         same(xb(0, c), sib, "sx0")
 
-    def b_cross():
-        arrive(xb(-1, c), "x1m")
-        arrive(xb(1, c), "x1p")
-        same(xb(-1, c, 0, HZ), xp, "x2m")
-        same(xb(1, c, HZ, HZ), xm, "x2p")
-        same(xb(-1, c), sib, "sx1m")
-        same(xb(1, c), sib, "sx1p")
-
-    def b_last():
-        arrive(xb(2, c, 0, HZ), "x2m")
-        arrive(xb(2, c, HZ, HZ), "x2p")
-        same(xb(2, c), sib, "sx2")
+    DOWN = (-1, -2, -3, 4)
+
+    def b_cross(i):
+        up, down = i, DOWN[i]
+        arrive(bp(up, -1), f"x1m{up}")
+        same(bp(up, -1), xp, f"x2m{up}")
+        arrive(bp(down, 1), f"x1p{down}")
+        same(bp(down, 1), xm, f"x2p{down}")
+        same(bp(up, -1), sib, "sx1m")
+        same(bp(down, 1), sib, "sx1p")
+
+    def b_collect(i):
+        up, down = i, DOWN[i]
+        arrive(bp(down, -1), f"x1m{down}")
+        arrive(bp(up, 1), f"x1p{up}")
+        same(bp(down, -1), sib, "sx1m")
+        same(bp(up, 1), sib, "sx1p")
+
+    def b_last(i):
+        up, down = i, DOWN[i]
+        arrive(bp(up, 2), f"x2m{up}")
+        arrive(bp(down, 2), f"x2p{down}")
+        same(bp(up, 2), sib, "sx2")
+        same(bp(down, 2), sib, "sx2")
 
     def b_done():
         arrive(xb(0, 1 - c), "sx0")
@@ -276,6 +326,8 @@
         d.wait()
     a_start()
     b_start()
+    bx_piece(0)
+    za_piece(0)
 
     @pl.when(c == 0)
     def _():
@@ -368,7 +420,7 @@
     a_one()
     b_step(1)
     slot_two[1]()
-    b_step(2)
+    a_two()
     slot_two[2]()
 
     @pl.when(c == 0)
@@ -384,15 +436,10 @@
     def _():
         copy_at(packs.at[2], packs.at[1], sib, "l1", S_ALT + 3).start()
 
-    b_step(3)
     arrive(docs.at[2], "d2")
     attend(2, 2, "full")
-    a_two()
-    b_turn()
-    arrive(packs.at[1], "l1")
-    arrive(docs.at[1], "d1")
-    before = jnp.where(sp >= 1, doc_column(1)[ROWS - 8 : ROWS, :], -1.0)
-    dcol[0:8, :] = jnp.broadcast_to(before, (8, 128))
+    b_step(2)
+    b_cross(0)
 
     @pl.when(c == 0)
     def _():
@@ -402,7 +449,13 @@
             zero_only.append(i)
             sends[i] = None
 
+    arrive(packs.at[1], "l1")
+    arrive(docs.at[1], "d1")
+    before = jnp.where(sp >= 1, doc_column(1)[ROWS - 8 : ROWS, :], -1.0)
+    dcol[0:8, :] = jnp.broadcast_to(before, (8, 128))
     attend(1, 1, "full")
+    b_step(3)
+    a_step(1)
     arrive(docs.at[3], "d3")
 
     @pl.when(c == 0)
@@ -414,7 +467,6 @@
         arrive(packs.at[3], "s3")
 
     attend(3, 3, "far", last=True)
-    a_step(1)
 
     def shared_sum(chunk, tag, ra, rb, pump_one, pump_two):
         f = chunk(wrap(y + 2, NY))
@@ -455,7 +507,19 @@
         return dot(att[...], op[:, pl.ds(pl.multiple_of(t * CH, CH), CH)])
 
     mark = len(sends)
-    total_one = shared_sum(head_share, "p", ra, rb, lambda: None, lambda: a_step(2))
+
+    def pump_early():
+        b_turn()
+        b_cross(1)
+        b_cross(2)
+
+    def pump_late():
+        a_step(2)
+        b_cross(3)
+        for i in range(4):
+            b_collect(i)
+
+    total_one = shared_sum(head_share, "p", ra, rb, pump_early, pump_late)
     m4[y] = (residual_scale * res[...].astype(F32) + total_one).astype(BF)
 
     def piece(dy, lo):
@@ -465,7 +529,6 @@
     same(piece(0, HALF), ym, "m1p1")
     same(piece(0, HALF), yp, "m1m1")
     same(piece(0, 0), ym, "m1p0")
-    b_cross()
     arrive(piece(-1, 0), "m1m0")
     same(piece(-1, 0), yp, "m2m")
     arrive(piece(1, HALF), "m1p1")
@@ -477,6 +540,8 @@
     a_step(3)
     arrive(piece(-1, HALF), "m1m1")
     arrive(piece(1, 0), "m1p0")
+    for i in range(4):
+        b_last(i)
     arrive(piece(2, 0), "m2m")
     arrive(piece(2, HALF), "m2p")
 
@@ -493,7 +558,6 @@
         return carry
 
     lax.fori_loop(0, ROWS // 32, norm_rows, 0)
-    b_last()
     a_last()
     b_done()
     a_done()
@@ -543,6 +607,8 @@
 
         lax.fori_loop(0, UNITS // 128, cols, 0)
 
+    for d in f_taps:
+        d.wait()
     conv_block(256)
     conv_block(128)
     arrive(stat.at[0], "t")
@@ -556,7 +622,27 @@
         return dot_nt(hid[:, 0:DA], da) + dot_nt(hid[:, DA:UNITS], db)
 
     settle(sends[mark : mark + 6])
-    total_two = shared_sum(unit_share, "u", ra2, rb2, lambda: None, lambda: None)
+    early = len(sends)
+
+    def settle_early():
+        settle(d for d in sends[:mark] if d is not None)
+        settle(sends[mark + 6 : early])
+        copy_at(docs.at[0], docs.at[1], sib, "d1", S_ALT + 1).wait_send()
+        copy_at(docs.at[0], docs.at[3], sib, "d3", S_ALT + 2).wait_send()
+        copy_at(packs.at[2], packs.at[3], sib, "s3", S_ALT + 3).wait_send()
+
+        @pl.when(c == 0)
+        def _():
+            copy_at(packs.at[0], packs.at[1], sib, "l1", S_ALT).wait_send()
+            for i, at in enumerate(zero_only):
+                part = quarter(3, 0, 0, QR if i < 2 else QR // 2)
+                copy_at(part, part, yp, "l3", at).wait_send()
+
+        @pl.when(c == 1)
+        def _():
+            copy_at(quarter(2, 0), quarter(3, 0), nexto, "l3", S_ALT).wait_send()
+
+    total_two = shared_sum(unit_share, "u", ra2, rb2, settle_early, lambda: None)
     mixed = (
         residual_scale * nf[:, pl.ds(pl.multiple_of(y * CH, CH), CH)].astype(F32) + total_two
     )
@@ -568,6 +654,7 @@
     same(stats.at[y], yp, "qm")
     same(stats.at[y], ym, "qp")
     same(stats.at[y], yy, "q2")
+    settle(sends[early:])
     arrive(stats.at[wrap(y - 1, NY)], "qm")
     arrive(stats.at[wrap(y + 1, NY)], "qp")
     arrive(stats.at[wrap(y + 2, NY)], "q2")
@@ -576,30 +663,7 @@
     s = back[:, 0:1] / D
     q = back[:, 1:2] / D
     r = lax.rsqrt(q - s * s + norm_eps)
-    out_ref[...] = ((own[...] - s) * r * gbs[y, 2:3, :] + gbs[y, 3:4, :]).astype(BF)
-    settle(d for d in sends[:mark] if d is not None)
-    settle(sends[mark + 6 :])
-    copy_at(docs.at[0], docs.at[1], sib, "d1", S_ALT + 1).wait_send()
-    copy_at(docs.at[0], docs.at[3], sib, "d3", S_ALT + 2).wait_send()
-    copy_at(packs.at[2], packs.at[3], sib, "s3", S_ALT + 3).wait_send()
-
-    @pl.when(c == 0)
-    def _():
-        copy_at(packs.at[0], packs.at[1], sib, "l1", S_ALT).wait_send()
-        for i, at in enumerate(zero_only):
-            part = quarter(3, 0, 0, QR if i < 2 else QR // 2)
-            copy_at(part, part, yp, "l3", at).wait_send()
-
-    @pl.when(c == 1)
-    def _():
-        copy_at(quarter(2, 0), quarter(3, 0), nexto, "l3", S_ALT).wait_send()
-
-
-def tables(positions):
-    frequencies = 1.0 / rope_base_freq ** (jnp.arange(0, ROPE, 2, dtype=jnp.float32) / ROPE)
-    angles = positions.astype(jnp.float32)[:, None] * jnp.tile(frequencies, 4)[None, :]
-    sign = jnp.where(jnp.arange(128) % ROPE < ROPE // 2, -1.0, 1.0).astype(jnp.float32)
-    return (jnp.cos(angles), jnp.sin(angles) * sign[None, :])
+    out_ref[...] = ((own[...] - s) * r * gb_ref[2:3, :] + gb_ref[3:4, :]).astype(BF)
 
 
 def local(
@@ -608,12 +672,8 @@
     norm2_gain, norm2_bias,
 ):
     rows = latent.shape[0]
-    positions = lax.axis_index("sp") * rows + jnp.arange(rows, dtype=jnp.int32)
-    cosine, sine = tables(positions)
-    doc = jnp.pad(doc_ids.astype(BF), (0, CH - rows))
-    none = jnp.zeros((3 * CH,), BF)
-    vectors = jnp.concatenate([norm1_gain, norm1_bias, norm2_gain, norm2_bias, doc, none])
-    vectors = vectors.astype(F32).reshape(8, CH)
+    turn = rope_base_freq ** (-np.arange(0, ROPE, 2, dtype=np.float64) / ROPE)
+    turn = jnp.asarray(np.tile(np.tile(turn, 4)[None], (8, 1)).astype(np.float32))
 
     anyspec = pl.BlockSpec(memory_space=pl.ANY)
     vspec = pl.BlockSpec(memory_space=pltpu.VMEM)
@@ -621,9 +681,21 @@
     return pl.pallas_call(
         layer_kernel,
         out_shape=jax.ShapeDtypeStruct((rows, CH), BF),
-        in_specs=[anyspec] * 10 + [vspec] * 6,
+        in_specs=[anyspec] * 19,
         out_specs=vspec,
         scratch_shapes=[
+            V((ROPE, ROWS), BF),
+            V((CH,), BF),
+            V((CH,), BF),
+            V((CH,), BF),
+            V((CH,), BF),
+            V((ROWS,), jnp.int32),
+            V((CONV, UNITS), BF),
+            V((CONV, UNITS), BF),
+            V((8, 128), F32),
+            V((8, CH), F32),
+            V((ROWS, 128), F32),
+            V((ROWS, 128), F32),
             V((4, ROWS, PACKW), BF),
             V((ROWS, 1024), BF),
             V((ROWS, CH), BF),
@@ -657,17 +729,17 @@
             V((ROWS, UNITS), BF),
             V((1, 8, 2 * UNITS), F32),
             V((NY, 8, ROWS), F32),
-            pltpu.SemaphoreType.DMA((11,)),
+            pltpu.SemaphoreType.DMA((24,)),
             pltpu.SemaphoreType.DMA((N_SEND,)),
             pltpu.SemaphoreType.DMA((N_RECV,)),
         ],
         compiler_params=pltpu.CompilerParams(
-            collective_id=0, has_side_effects=True, vmem_limit_bytes=60 * 1024 * 1024
+            collective_id=0, has_side_effects=True, vmem_limit_bytes=54 * 1024 * 1024
         ),
     )(
         latent, query_nope, query_rope, key_up, value_up, out_proj, residual,
-        ffn_gate, ffn_value, ffn_down.T, rope_key.T, cosine, sine,
-        vectors, conv_gate, conv_value,
+        ffn_gate, ffn_value, ffn_down.T, rope_key.T, norm1_gain, norm1_bias, norm2_gain, norm2_bias,
+        doc_ids, conv_gate, conv_value, turn,
     )
 
 

time: 119 us -> 108 us (0.908)
  the two profiles are of different devices: /device:TPU:64 before, /device:TPU:6 now
where the time goes in v3:
time: 108 us
  Pallas kernels  107 us (99%)
  local copies, waits for them, and re-layouts  1.77 us (2%)
    pallas_call x1, Pallas kernels, local(): pl.pallas_call(layer_kernel, out_shape=jax.ShapeDtypeStruct((rows, CH), B...  107 us

profile of v3, /device:TPU:6, one launch (start us, length us, event | category | flops | bytes accessed | tf_op | source)
XLA Modules:
  0.0 108.3 jit_solution(844115993420974149)
XLA Ops:
  0.0 106.5 %shard_map.181 = bf16[384,512]{1,0:T(8,128)(2,1)} custom-call(bf16[384,512]{1,0:T(8,128)(2,1)} %lat_h.1, bf16[384,1024]{1,0:T(8,128)(2,1)} %qn_h.1, bf16[384,512]{1,0:T(8,128)(2,1)} %qr_h.1, bf16[512,1024]{1,0:T(8,128)(2,1)} %kup_h.1, bf16[512,1024]{1,0:T(8,128)(2,1)} %vup_h.1, bf16[1024,2048]{1,0:T(8,128)(2,1)} %op_h.1, bf16[384,512]{1,0:T(8,128)(2,1)} %res_h.1, ...), custom_call_target="tpu_custom_call" | custom-call | tf_op jit(solution)/shard_map/pallas_call | solution.py:681
  106.5 1.8 %copy.21 = bf16[384,512]{1,0:T(8,128)(2,1)} copy(bf16[384,512]{1,0:T(8,128)(2,1)} %shard_map.181) | data formatting | bytes 786432

commit v4 on v3

--- a/solution.py
+++ b/solution.py
@@ -22,13 +22,14 @@
 NX, NZ, NY = 4, 8, 4
 ROWS = 384
 HALF = ROWS // 2
+LEAD = 16
 CH = 512
 UNITS = 1408
 DA = 256
 LA = DA + UNITS
 LW = 3 * UNITS
 PACKW = 640
-GROUP = 4
+GROUP = 8
 N_SEND = 128
 N_RECV = 128
 S_ALT = N_SEND - 4
@@ -51,7 +52,7 @@
     out_ref,
     key_ref, v0, v1, v2, v3, doc_ref, cg_ref, cv_ref, freq_ref, gb_ref, cos_ref, sin_ref,
     packs, qn, qraw, qr, kup, vup, op, res, w, gbs, att, acc, mrun, lrun, dcol, docs, bias,
-    sa, sp_buf, sm_buf, pfp, pfm, own, ra, rb, ra2, rb2, m4, nf, gv, hid, stat, stats,
+    sa, sp_buf, sm_buf, pfp, pfm, own, ra, rb, ra2, rb2, m4, nf, gv, hid, before_rows, stats,
     lsem, ssem, rsem,
 ):
     sp = lax.axis_index("sp")
@@ -129,7 +130,7 @@
     cos_ref[...] = jnp.cos(angle)
     sin_ref[...] = jnp.where(front, -1.0, 1.0) * jnp.sin(angle)
     key = key_ref[...].astype(F32)
-    packs[0, :, 512:640] = turned(jnp.concatenate([key, key], axis=0).T).astype(BF)
+    packs[0, :, 512:640] = (turned(jnp.concatenate([key, key], axis=0).T) * SCALE2).astype(BF)
     docs[0] = jnp.broadcast_to(doc_ref[...].astype(F32).reshape(1, ROWS), (8, ROWS))
     gb_ref[...] = jnp.concatenate(
         [v[...].astype(F32).reshape(1, CH) for v in (v0, v1, v2, v3)] + [jnp.zeros((4, CH), F32)], axis=0
@@ -369,26 +370,39 @@
                 lanes.append(pl.ds(pl.multiple_of(h * 128, 128), 128))
                 if not first:
                     states.append((mrun[h], lrun[h], acc[h]))
+            pairs = {}
+
+            def keys(i):
+                both = pl.ds(pl.multiple_of((group * GROUP + 2 * i) * 128, 256), 256)
+                pairs[i] = (
+                    (dot(lat, kup[:, both]) * SCALE2).astype(BF),
+                    dot(lat, vup[:, both]).astype(BF),
+                )
+
+            def score(hh):
+                k2 = pairs[hh // 2][0][:, hh % 2 * 128 : hh % 2 * 128 + 128]
+                q = jnp.concatenate([qn[:, lanes[hh]], qr[:, lanes[hh]]], axis=1)
+                return dot_nt(q, jnp.concatenate([k2, kr], axis=1)) + bias[...]
+
+            keys(0)
+            ahead = score(0)
             for hh in range(GROUP):
-                if hh % 2 == 0:
-                    both = pl.ds(pl.multiple_of((group * GROUP + hh) * 128, 256), 256)
-                    k2 = dot(lat, kup[:, both]).astype(BF)
-                    v2 = dot(lat, vup[:, both]).astype(BF)
-                part = slice(hh % 2 * 128, hh % 2 * 128 + 128)
-                kk = jnp.concatenate([k2[:, part], kr], axis=1)
-                vv = jnp.concatenate([v2[:, part], ones], axis=1)
-                q = jnp.concatenate([qn[:, lanes[hh]], qr[:, lanes[hh]]], axis=1)
-                s = dot_nt(q, kk) + bias[...]
+                s = ahead
+                if hh % 2 == 0 and hh + 2 < GROUP:
+                    keys(hh // 2 + 1)
+                if hh + 1 < GROUP:
+                    ahead = score(hh + 1)
+                v2 = pairs[hh // 2][1][:, hh % 2 * 128 : hh % 2 * 128 + 128]
                 mx = jnp.max(s, axis=1, keepdims=True)
                 if first:
                     mnew = jnp.broadcast_to(mx, (ROWS, 128))
                 else:
                     mnew = jnp.maximum(states[hh][0], mx)
-                p = jnp.exp2((s - mnew[:, 0:1]) * SCALE2)
-                o = dot(p.astype(BF), vv)
+                p = jnp.exp2(s - mnew[:, 0:1])
+                o = dot(p.astype(BF), jnp.concatenate([v2, ones], axis=1))
                 o, total = o[:, 0:128], o[:, 128:256]
                 if not first:
-                    alpha = jnp.exp2((states[hh][0] - mnew) * SCALE2)
+                    alpha = jnp.exp2(states[hh][0] - mnew)
                     total = states[hh][1] * alpha + total
                     o = states[hh][2] * alpha + o
                 results.append((mnew, total, o))
@@ -468,32 +482,36 @@
 
     attend(3, 3, "far", last=True)
 
-    def shared_sum(chunk, tag, ra, rb, pump_one, pump_two):
-        f = chunk(wrap(y + 2, NY))
-        sa[...] = f.astype(BF)
-        send(sa.at[pl.ds(0, HALF)], ra.at[0], yp, tag + "am")
-        send(sa.at[pl.ds(HALF, HALF)], ra.at[1], ym, tag + "ap")
-        f = chunk(wrap(y + 1, NY))
+    UP, LOW = pl.ds(0, HALF), pl.ds(HALF, HALF)
+
+    def far_all(chunk, tag, ra):
+        sa[...] = chunk(wrap(y + 2, NY), pl.ds(0, ROWS)).astype(BF)
+        send(sa.at[UP], ra.at[0], yp, tag + "am")
+        send(sa.at[LOW], ra.at[1], ym, tag + "ap")
+
+    def near_all(chunk, tag, rb):
+        f = chunk(wrap(y + 1, NY), pl.ds(0, ROWS))
         pfp[...] = f[:HALF]
-        sp_buf[pl.ds(HALF, HALF), :] = f[HALF:].astype(BF)
-        send(sp_buf.at[pl.ds(HALF, HALF)], rb.at[0, pl.ds(HALF, HALF)], yp, tag + "bm1")
-        f = chunk(wrap(y - 1, NY))
+        sp_buf[LOW, :] = f[HALF:].astype(BF)
+        send(sp_buf.at[LOW], rb.at[0, LOW], yp, tag + "bm1")
+        f = chunk(wrap(y - 1, NY), pl.ds(0, ROWS))
         pfm[...] = f[HALF:]
-        sm_buf[pl.ds(0, HALF), :] = f[:HALF].astype(BF)
-        send(sm_buf.at[pl.ds(0, HALF)], rb.at[1, pl.ds(0, HALF)], ym, tag + "bp0")
-        own[...] = chunk(y)
-        pump_one()
+        sm_buf[UP, :] = f[:HALF].astype(BF)
+        send(sm_buf.at[UP], rb.at[1, UP], ym, tag + "bp0")
+
+    def forward(tag, ra, rb):
         arrive(ra.at[0], tag + "am")
-        sp_buf[pl.ds(0, HALF), :] = (pfp[...] + ra[0].astype(F32)).astype(BF)
-        send(sp_buf.at[pl.ds(0, HALF)], rb.at[0, pl.ds(0, HALF)], yp, tag + "bm0")
+        sp_buf[UP, :] = (pfp[...] + ra[0].astype(F32)).astype(BF)
+        send(sp_buf.at[UP], rb.at[0, UP], yp, tag + "bm0")
         arrive(ra.at[1], tag + "ap")
-        sm_buf[pl.ds(HALF, HALF), :] = (pfm[...] + ra[1].astype(F32)).astype(BF)
-        send(sm_buf.at[pl.ds(HALF, HALF)], rb.at[1, pl.ds(HALF, HALF)], ym, tag + "bp1")
-        pump_two()
-        arrive(rb.at[0, pl.ds(HALF, HALF)], tag + "bm1")
-        arrive(rb.at[1, pl.ds(0, HALF)], tag + "bp0")
-        arrive(rb.at[0, pl.ds(0, HALF)], tag + "bm0")
-        arrive(rb.at[1, pl.ds(HALF, HALF)], tag + "bp1")
+        sm_buf[LOW, :] = (pfm[...] + ra[1].astype(F32)).astype(BF)
+        send(sm_buf.at[LOW], rb.at[1, LOW], ym, tag + "bp1")
+
+    def collected(tag, rb):
+        arrive(rb.at[0, LOW], tag + "bm1")
+        arrive(rb.at[1, UP], tag + "bp0")
+        arrive(rb.at[0, UP], tag + "bm0")
+        arrive(rb.at[1, LOW], tag + "bp1")
         return own[...] + rb[0].astype(F32) + rb[1].astype(F32)
 
     def settle(ds):
@@ -503,23 +521,20 @@
     f_op.wait()
     f_res.wait()
 
-    def head_share(t):
-        return dot(att[...], op[:, pl.ds(pl.multiple_of(t * CH, CH), CH)])
+    def head_share(t, rows):
+        return dot(att[rows, :], op[:, pl.ds(pl.multiple_of(t * CH, CH), CH)])
 
     mark = len(sends)
 
-    def pump_early():
-        b_turn()
-        b_cross(1)
-        b_cross(2)
-
-    def pump_late():
-        a_step(2)
-        b_cross(3)
-        for i in range(4):
-            b_collect(i)
-
-    total_one = shared_sum(head_share, "p", ra, rb, pump_early, pump_late)
+    far_all(head_share, "p", ra)
+    near_all(head_share, "p", rb)
+    own[...] = head_share(y, pl.ds(0, ROWS))
+    b_turn()
+    forward("p", ra, rb)
+    b_cross(1)
+    b_cross(2)
+    a_step(2)
+    total_one = collected("p", rb)
     m4[y] = (residual_scale * res[...].astype(F32) + total_one).astype(BF)
 
     def piece(dy, lo):
@@ -529,6 +544,7 @@
     same(piece(0, HALF), ym, "m1p1")
     same(piece(0, HALF), yp, "m1m1")
     same(piece(0, 0), ym, "m1p0")
+    b_cross(3)
     arrive(piece(-1, 0), "m1m0")
     same(piece(-1, 0), yp, "m2m")
     arrive(piece(1, HALF), "m1p1")
@@ -538,6 +554,8 @@
     arrive(gbs.at[wrap(y + 2, NY)], "g2")
     gbs[y] = gb_ref[...]
     a_step(3)
+    for i in range(4):
+        b_collect(i)
     arrive(piece(-1, HALF), "m1m1")
     arrive(piece(1, 0), "m1p0")
     for i in range(4):
@@ -545,81 +563,83 @@
     arrive(piece(2, 0), "m2m")
     arrive(piece(2, HALF), "m2p")
 
-    def norm_rows(i, carry):
-        rows = pl.ds(pl.multiple_of(i * 32, 32), 32)
-        parts = [m4[t, rows, :].astype(F32) for t in range(NY)]
+    def norm_of(src, rows, out_rows):
+        parts = [src[t, rows, :].astype(F32) for t in range(NY)]
         s = sum(jnp.sum(v, axis=1, keepdims=True) for v in parts) / D
         q = sum(jnp.sum(v * v, axis=1, keepdims=True) for v in parts) / D
         r = lax.rsqrt(q - s * s + norm_eps)
         for t in range(NY):
-            nf[rows, t * CH : (t + 1) * CH] = (
+            nf[out_rows, t * CH : (t + 1) * CH] = (
                 (parts[t] - s) * r * gbs[t, 0:1, :] + gbs[t, 1:2, :]
             ).astype(BF)
+
+    def norm_rows(i, carry):
+        first = pl.multiple_of(i * 32, 32)
+        norm_of(m4, pl.ds(first, 32), pl.ds(pl.multiple_of(first + LEAD, 16), 32))
         return carry
 
+    tail = m4.at[:, pl.ds(ROWS - LEAD, LEAD), :]
+    copy_to(tail, before_rows, sib, "t")
+    tail_at = len(sends) - 1
+
+    @pl.when(c == 0)
+    def _():
+        copy_at(tail, before_rows, sib, "t", tail_at).start()
+
+    @pl.when(c == 1)
+    def _():
+        copy_at(tail, before_rows, nexto, "t", tail_at).start()
+
+    a_last()
     lax.fori_loop(0, ROWS // 32, norm_rows, 0)
-    a_last()
     b_done()
     a_done()
 
-    def up(j, carry):
-        lanes = pl.ds(pl.multiple_of(DA + j * 256, 128), 256)
-        f = dot(nf[...], w[:, :, :, :, lanes].reshape(D, 256))
-        gv[8 : 8 + ROWS, pl.ds(pl.multiple_of(j * 256, 256), 256)] = f
-        return carry
-
-    lax.fori_loop(0, 2 * UNITS // 256, up, 0)
-    tail = pl.ds(ROWS, 8)
-
-    to_sib = copy_to(gv.at[tail], stat.at[0], sib, "t")
-    to_next = pltpu.make_async_remote_copy(
-        src_ref=gv.at[tail], dst_ref=stat.at[0], send_sem=ssem.at[len(sends) - 1],
-        recv_sem=rsem.at[rid("t")], device_id=nexto, device_id_type=MESH,
-    )
-
-    @pl.when(c == 0)
-    def _():
-        to_sib.start()
-
-    @pl.when(c == 1)
-    def _():
-        to_next.start()
-
-    def conv_block(r0):
-        here = dcol[8 + r0 : 8 + r0 + 128, :]
-        one = (dcol[7 + r0 : 7 + r0 + 128, :] == here).astype(F32)
-        two = (dcol[6 + r0 : 6 + r0 + 128, :] == here).astype(F32)
-
-        def cols(j, carry):
-            def mix(taps, base):
-                lanes = pl.ds(pl.multiple_of(base + j * 128, 128), 128)
-                a0 = gv[6 + r0 : 6 + r0 + 128, lanes]
-                a1 = gv[7 + r0 : 7 + r0 + 128, lanes]
-                a2 = gv[8 + r0 : 8 + r0 + 128, lanes]
-                t = taps[:, pl.ds(pl.multiple_of(j * 128, 128), 128)].astype(F32)
-                return t[0:1] * a0 * two + t[1:2] * a1 * one + t[2:3] * a2
-
-            g = mix(cg_ref, 0)
-            v = mix(cv_ref, UNITS)
-            act = 0.5 * g * (1.0 + jnp.tanh(0.7978845608028654 * (g + 0.044715 * (g * g * g))))
-            hid[r0 : r0 + 128, pl.ds(pl.multiple_of(j * 128, 128), 128)] = (v * act).astype(BF)
-            return carry
-
-        lax.fori_loop(0, UNITS // 128, cols, 0)
-
+    arrive(before_rows, "t")
+    norm_of(before_rows, pl.ds(0, LEAD), pl.ds(0, LEAD))
     for d in f_taps:
         d.wait()
-    conv_block(256)
-    conv_block(128)
-    arrive(stat.at[0], "t")
-    gv[0:8, :] = jnp.where(sp >= 1, stat[0], 0.0)
-    conv_block(0)
-
-    def unit_share(t):
-        rows = pl.ds(2 * t, 2)
-        da = w[rows, :, :, :, 0:DA].reshape(CH, DA)
-        db = w[rows, :, :, :, LA + UNITS : LW].reshape(CH, UNITS - DA)
-        return dot_nt(hid[:, 0:DA], da) + dot_nt(hid[:, DA:UNITS], db)
+
+    def block(base, j):
+        return pl.ds(pl.multiple_of(base + j * 128, 128), 128)
+
+    def up(j):
+        both = jnp.concatenate([w[:, :, :, :, block(DA, j)], w[:, :, :, :, block(LA, j)]], axis=4)
+        f = dot(nf[...], both.reshape(D, 256))
+        gv[:, block(0, j)] = f[:, 0:128]
+        gv[:, block(UNITS, j)] = f[:, 128:256]
+
+    def conv(j):
+        here = dcol[8 : 8 + ROWS, :]
+        near = (dcol[7 : 7 + ROWS, :] == here).astype(F32)
+        far = (dcol[6 : 6 + ROWS, :] == here).astype(F32)
+
+        def mix(taps, base):
+            a0 = gv[LEAD - 2 : LEAD - 2 + ROWS, block(base, j)]
+            a1 = gv[LEAD - 1 : LEAD - 1 + ROWS, block(base, j)]
+            a2 = gv[LEAD : LEAD + ROWS, block(base, j)]
+            t = taps[:, block(0, j)].astype(F32)
+            return t[0:1] * a0 * far + t[1:2] * a1 * near + t[2:3] * a2
+
+        g = mix(cg_ref, 0)
+        v = mix(cv_ref, UNITS)
+        act = 0.5 * g * (1.0 + jnp.tanh(0.7978845608028654 * (g + 0.044715 * (g * g * g))))
+        hid[:, block(0, j)] = (v * act).astype(BF)
+
+    def step(j, carry):
+        conv(j - 1)
+        up(j)
+        return carry
+
+    up(0)
+    lax.fori_loop(1, UNITS // 128, step, 0)
+    conv(UNITS // 128 - 1)
+
+    def unit_share(t, rows):
+        part = pl.ds(2 * t, 2)
+        da = w[part, :, :, :, 0:DA].reshape(CH, DA)
+        db = w[part, :, :, :, LA + UNITS : LW].reshape(CH, UNITS - DA)
+        return dot_nt(hid[rows, 0:DA], da) + dot_nt(hid[rows, DA:UNITS], db)
 
     settle(sends[mark : mark + 6])
     early = len(sends)
@@ -642,9 +662,14 @@
         def _():
             copy_at(quarter(2, 0), quarter(3, 0), nexto, "l3", S_ALT).wait_send()
 
-    total_two = shared_sum(unit_share, "u", ra2, rb2, settle_early, lambda: None)
+    far_all(unit_share, "u", ra2)
+    near_all(unit_share, "u", rb2)
+    own[...] = unit_share(y, pl.ds(0, ROWS))
+    settle_early()
+    forward("u", ra2, rb2)
+    total_two = collected("u", rb2)
     mixed = (
-        residual_scale * nf[:, pl.ds(pl.multiple_of(y * CH, CH), CH)].astype(F32) + total_two
+        residual_scale * nf[LEAD : LEAD + ROWS, pl.ds(pl.multiple_of(y * CH, CH), CH)].astype(F32) + total_two
     )
     own[...] = mixed
     s = jnp.sum(mixed, axis=1, keepdims=True)
@@ -724,10 +749,10 @@
             V((2, HALF, CH), BF),
             V((2, ROWS, CH), BF),
             V((NY, ROWS, CH), BF),
-            V((ROWS, D), BF),
-            V((8 + ROWS, 2 * UNITS), F32),
+            V((LEAD + ROWS, D), BF),
+            V((LEAD + ROWS, 2 * UNITS), F32),
             V((ROWS, UNITS), BF),
-            V((1, 8, 2 * UNITS), F32),
+            V((NY, LEAD, CH), BF),
             V((NY, 8, ROWS), F32),
             pltpu.SemaphoreType.DMA((24,)),
             pltpu.SemaphoreType.DMA((N_SEND,)),

time: 108 us -> 106 us (0.981)
  Pallas kernels: 107 us -> 104 us
    pallas_call x1, Pallas kernels: 107 us -> 104 us  [local(): pl.pallas_call(layer_kernel, out_shape=jax.ShapeDtypeStruct((rows, CH), B...]
where the time goes in v4:
time: 106 us
  Pallas kernels  104 us (98%)
  local copies, waits for them, and re-layouts  1.77 us (2%)
    pallas_call x1, Pallas kernels, local(): pl.pallas_call(layer_kernel, out_shape=jax.ShapeDtypeStruct((rows, CH), B...  104 us

profile of v4, /device:TPU:6, one launch (start us, length us, event | category | flops | bytes accessed | tf_op | source)
XLA Modules:
  0.0 105.5 jit_solution(15630138877931574695)
XLA Ops:
  0.0 103.8 %shard_map.181 = bf16[384,512]{1,0:T(8,128)(2,1)} custom-call(bf16[384,512]{1,0:T(8,128)(2,1)} %lat_h.1, bf16[384,1024]{1,0:T(8,128)(2,1)} %qn_h.1, bf16[384,512]{1,0:T(8,128)(2,1)} %qr_h.1, bf16[512,1024]{1,0:T(8,128)(2,1)} %kup_h.1, bf16[512,1024]{1,0:T(8,128)(2,1)} %vup_h.1, bf16[1024,2048]{1,0:T(8,128)(2,1)} %op_h.1, bf16[384,512]{1,0:T(8,128)(2,1)} %res_h.1, ...), custom_call_target="tpu_custom_call" | custom-call | tf_op jit(solution)/shard_map/pallas_call | solution.py:706
  103.8 1.8 %copy.21 = bf16[384,512]{1,0:T(8,128)(2,1)} copy(bf16[384,512]{1,0:T(8,128)(2,1)} %shard_map.181) | data formatting | bytes 786432

commit v5 on v4

--- a/solution.py
+++ b/solution.py
@@ -23,6 +23,7 @@
 ROWS = 384
 HALF = ROWS // 2
 LEAD = 16
+PARTS = 4
 CH = 512
 UNITS = 1408
 DA = 256
@@ -432,9 +433,8 @@
         copy_at(quarter(2, 0), quarter(3, 0), nexto, "l3", S_ALT).start()
 
     a_one()
+    slot_two[1]()
     b_step(1)
-    slot_two[1]()
-    a_two()
     slot_two[2]()
 
     @pl.when(c == 0)
@@ -452,6 +452,7 @@
 
     arrive(docs.at[2], "d2")
     attend(2, 2, "full")
+    a_two()
     b_step(2)
     b_cross(0)
 
@@ -468,7 +469,6 @@
     before = jnp.where(sp >= 1, doc_column(1)[ROWS - 8 : ROWS, :], -1.0)
     dcol[0:8, :] = jnp.broadcast_to(before, (8, 128))
     attend(1, 1, "full")
-    b_step(3)
     a_step(1)
     arrive(docs.at[3], "d3")
 
@@ -529,8 +529,9 @@
     far_all(head_share, "p", ra)
     near_all(head_share, "p", rb)
     own[...] = head_share(y, pl.ds(0, ROWS))
+    b_step(3)
+    forward("p", ra, rb)
     b_turn()
-    forward("p", ra, rb)
     b_cross(1)
     b_cross(2)
     a_step(2)
@@ -603,37 +604,57 @@
     def block(base, j):
         return pl.ds(pl.multiple_of(base + j * 128, 128), 128)
 
-    def up(j):
-        both = jnp.concatenate([w[:, :, :, :, block(DA, j)], w[:, :, :, :, block(LA, j)]], axis=4)
-        f = dot(nf[...], both.reshape(D, 256))
+    KC = D // PARTS
+    RC = ROWS // PARTS
+
+    def up_part(j, i):
+        zs = slice(i * NZ // PARTS, (i + 1) * NZ // PARTS)
+        both = jnp.concatenate(
+            [w[zs, :, :, :, block(DA, j)], w[zs, :, :, :, block(LA, j)]], axis=4
+        )
+        return dot(nf[:, i * KC : (i + 1) * KC], both.reshape(KC, 256))
+
+    def keep(j, f):
         gv[:, block(0, j)] = f[:, 0:128]
         gv[:, block(UNITS, j)] = f[:, 128:256]
 
-    def conv(j):
-        here = dcol[8 : 8 + ROWS, :]
-        near = (dcol[7 : 7 + ROWS, :] == here).astype(F32)
-        far = (dcol[6 : 6 + ROWS, :] == here).astype(F32)
+    def conv_part(j, i):
+        r0 = i * RC
+        here = dcol[8 + r0 : 8 + r0 + RC, :]
+        near = (dcol[7 + r0 : 7 + r0 + RC, :] == here).astype(F32)
+        far = (dcol[6 + r0 : 6 + r0 + RC, :] == here).astype(F32)
 
         def mix(taps, base):
-            a0 = gv[LEAD - 2 : LEAD - 2 + ROWS, block(base, j)]
-            a1 = gv[LEAD - 1 : LEAD - 1 + ROWS, block(base, j)]
-            a2 = gv[LEAD : LEAD + ROWS, block(base, j)]
+            lo = LEAD + r0
+            a0 = gv[lo - 2 : lo - 2 + RC, block(base, j)]
+            a1 = gv[lo - 1 : lo - 1 + RC, block(base, j)]
+            a2 = gv[lo : lo + RC, block(base, j)]
             t = taps[:, block(0, j)].astype(F32)
             return t[0:1] * a0 * far + t[1:2] * a1 * near + t[2:3] * a2
 
         g = mix(cg_ref, 0)
         v = mix(cv_ref, UNITS)
         act = 0.5 * g * (1.0 + jnp.tanh(0.7978845608028654 * (g + 0.044715 * (g * g * g))))
-        hid[:, block(0, j)] = (v * act).astype(BF)
+        return (v * act).astype(BF)
 
     def step(j, carry):
-        conv(j - 1)
-        up(j)
+        f, done = None, []
+        for i in range(PARTS):
+            part = up_part(j, i)
+            f = part if f is None else f + part
+            done.append(conv_part(j - 1, i))
+        for i in range(PARTS):
+            hid[i * RC : (i + 1) * RC, block(0, j - 1)] = done[i]
+        keep(j, f)
         return carry
 
-    up(0)
+    f = up_part(0, 0)
+    for i in range(1, PARTS):
+        f = f + up_part(0, i)
+    keep(0, f)
     lax.fori_loop(1, UNITS // 128, step, 0)
-    conv(UNITS // 128 - 1)
+    for i in range(PARTS):
+        hid[i * RC : (i + 1) * RC, block(0, UNITS // 128 - 1)] = conv_part(UNITS // 128 - 1, i)
 
     def unit_share(t, rows):
         part = pl.ds(2 * t, 2)

time: 106 us -> 99.2 us (0.936)
  Pallas kernels: 104 us -> 97.3 us
    pallas_call x1, Pallas kernels: 104 us -> 97.3 us  [local(): pl.pallas_call(layer_kernel, out_shape=jax.ShapeDtypeStruct((rows, CH), B...]
where the time goes in v5:
time: 99.2 us; the launch traced here: 99.1 us
  Pallas kernels  97.3 us (98%)
  local copies, waits for them, and re-layouts  1.77 us (2%)
    pallas_call x1, Pallas kernels, local(): pl.pallas_call(layer_kernel, out_shape=jax.ShapeDtypeStruct((rows, CH), B...  97.3 us

profile of v5, /device:TPU:6, one launch (start us, length us, event | category | flops | bytes accessed | tf_op | source)
XLA Modules:
  0.0 99.1 jit_solution(6797670303473347158)
XLA Ops:
  0.0 97.3 %shard_map.181 = bf16[384,512]{1,0:T(8,128)(2,1)} custom-call(bf16[384,512]{1,0:T(8,128)(2,1)} %lat_h.1, bf16[384,1024]{1,0:T(8,128)(2,1)} %qn_h.1, bf16[384,512]{1,0:T(8,128)(2,1)} %qr_h.1, bf16[512,1024]{1,0:T(8,128)(2,1)} %kup_h.1, bf16[512,1024]{1,0:T(8,128)(2,1)} %vup_h.1, bf16[1024,2048]{1,0:T(8,128)(2,1)} %op_h.1, bf16[384,512]{1,0:T(8,128)(2,1)} %res_h.1, ...), custom_call_target="tpu_custom_call" | custom-call | tf_op jit(solution)/shard_map/pallas_call | solution.py:727
  97.3 1.8 %copy.21 = bf16[384,512]{1,0:T(8,128)(2,1)} copy(bf16[384,512]{1,0:T(8,128)(2,1)} %shard_map.181) | data formatting | bytes 786432

commit v6 on v5

--- a/solution.py
+++ b/solution.py
@@ -591,8 +591,8 @@
     def _():
         copy_at(tail, before_rows, nexto, "t", tail_at).start()
 
+    lax.fori_loop(0, ROWS // 32, norm_rows, 0)
     a_last()
-    lax.fori_loop(0, ROWS // 32, norm_rows, 0)
     b_done()
     a_done()
 

time: 99.2 us -> 101 us (1.018)
  the two profiles are of different devices: /device:TPU:6 before, /device:TPU:1 now
where the time goes in v6:
time: 101 us
  Pallas kernels  98.9 us (98%)
  local copies, waits for them, and re-layouts  1.77 us (2%)
    pallas_call x1, Pallas kernels, local(): pl.pallas_call(layer_kernel, out_shape=jax.ShapeDtypeStruct((rows, CH), B...  98.9 us

profile of v6, /device:TPU:1, one launch (start us, length us, event | category | flops | bytes accessed | tf_op | source)
XLA Modules:
  0.0 100.7 jit_solution(562109484121277598)
XLA Ops:
  0.0 98.9 %shard_map.181 = bf16[384,512]{1,0:T(8,128)(2,1)} custom-call(bf16[384,512]{1,0:T(8,128)(2,1)} %lat_h.1, bf16[384,1024]{1,0:T(8,128)(2,1)} %qn_h.1, bf16[384,512]{1,0:T(8,128)(2,1)} %qr_h.1, bf16[512,1024]{1,0:T(8,128)(2,1)} %kup_h.1, bf16[512,1024]{1,0:T(8,128)(2,1)} %vup_h.1, bf16[1024,2048]{1,0:T(8,128)(2,1)} %op_h.1, bf16[384,512]{1,0:T(8,128)(2,1)} %res_h.1, ...), custom_call_target="tpu_custom_call" | custom-call | tf_op jit(solution)/shard_map/pallas_call | solution.py:727
  98.9 1.8 %copy.21 = bf16[384,512]{1,0:T(8,128)(2,1)} copy(bf16[384,512]{1,0:T(8,128)(2,1)} %shard_map.181) | data formatting | bytes 786432
